TPU v7x, 32 devices: a whole 2x2x4 slice. The times are simulated.
32 devices in a mesh: sp: 4 (over y, x), tp: 8 (over z, core).
Axes of the slice: x: 2, y: 2, z: 4, core: 2. Of those that a mesh axis runs over, the one named last changes fastest.
Arguments:
- queries: bfloat16 [4096, 1024], P('sp', 'tp'), may hold values from -18 to 18
- keys: bfloat16 [4096, 256], P('sp'), may hold values from -18 to 18
- values: bfloat16 [4096, 256], P('sp'), may hold values from -6 to 6
- sink_logits: float32 [16], P('tp'), may hold values from 3 to 7
- w_out: bfloat16 [1024, 2048], P('tp'), may hold values from -1.5 to 1.5
- residual: bfloat16 [4096, 2048], P(('sp', 'tp')), may hold values from -6 to 6
- norm_gain: float32 [2048], replicated, may hold values from 0.1 to 1.9
- expert_ids: int32 [4096, 4], P('sp'), may hold values from 0 to 15, all different within a row; in each aligned block of 1024 rows (0 to 1023, 1024 to 2047, ...) at most 512 rows name the same one
- expert_weights: float32 [4096, 4], P('sp'), may hold values from 0.1 to 1.5
- w_gate: bfloat16 [32, 768, 2048], P(('sp', 'tp')), may hold values from -0.125 to 0.125
- w_up: bfloat16 [32, 768, 2048], P(('sp', 'tp')), may hold values from -0.125 to 0.125
- w_down: bfloat16 [32, 768, 2048], P(('sp', 'tp')), may hold values from -0.15625 to 0.15625
- shared_gate: bfloat16 [512, 2048], P('tp'), may hold values from -0.125 to 0.125
- shared_up: bfloat16 [512, 2048], P('tp'), may hold values from -0.125 to 0.125
- shared_down: bfloat16 [512, 2048], P('tp'), may hold values from -0.25 to 0.25
Outputs:
- layer_out: bfloat16 [4096, 2048], P(('sp', 'tp'))
Inputs may be any that keep to these rules, and one draw needn't show every extreme that they name: `expert_ids`: each row names 4 different experts; in each aligned block of 1024 rows no expert is named by more than 512 rows.
All inputs are finite; a program needn't handle non-finite values.
Results may differ from a plain program's by a relative error of at most 0.02.
Values may be sent and summed in bfloat16 or wider, within the bound.
No kernel may reach another device: no remote copies, remote signals or barrier semaphores. Data moves between devices by JAX's collectives and lax.ppermute only.
A program may use at most 128 MiB of HBM per device.

v0:
```python
import jax
import jax.numpy as jnp
from jax import lax
from jax.experimental import pallas as pl
from jax.experimental.pallas import tpu as pltpu
from jax.sharding import PartitionSpec as P

HD = 64
GROUP = 4
WINDOW = 128
TOPK = 4
CHUNKS = 2
AHEAD = 2


WHOLE = pl.BlockSpec(memory_space=pltpu.VMEM)
ROOMY = pltpu.CompilerParams(vmem_limit_bytes=40 * 2**20)


def shifted(block, axis, distance):
    devices = range(lax.axis_size(axis))
    route = [(i - distance, i) for i in devices if i - distance in devices]
    return lax.ppermute(block, axis, route)


def peer(x, axis, step):
    if step == 0:
        return x
    count = lax.axis_size(axis)
    return lax.ppermute(x, axis, [(i, i ^ step) for i in range(count)])


def attention(queries, keys, values, sink_logits):
    seq_rows = queries.shape[0]
    local_heads = queries.shape[1] // HD
    kv_start = lax.axis_index("tp") * local_heads // GROUP * HD
    key_cols = lax.dynamic_slice_in_dim(keys, kv_start, HD, 1)
    value_cols = lax.dynamic_slice_in_dim(values, kv_start, HD, 1)
    rim = jnp.concatenate(
        [key_cols[seq_rows - WINDOW :], value_cols[seq_rows - WINDOW :]], axis=1
    )
    rim = shifted(rim, "sp", 1)
    rim_keys, rim_values = rim[:, :HD], rim[:, HD:]
    num_blocks = seq_rows // WINDOW
    key_blocks = key_cols.reshape(num_blocks, WINDOW, HD)
    value_blocks = value_cols.reshape(num_blocks, WINDOW, HD)
    keys_ext = jnp.concatenate(
        [jnp.concatenate([rim_keys[None], key_blocks[:-1]], axis=0), key_blocks], axis=1
    )
    values_ext = jnp.concatenate(
        [jnp.concatenate([rim_values[None], value_blocks[:-1]], axis=0), value_blocks], axis=1
    )
    query_blocks = queries.reshape(num_blocks, WINDOW, local_heads, HD)
    scores = jnp.einsum(
        "nqhd,nsd->nhqs", query_blocks, keys_ext, preferred_element_type=jnp.float32
    ) * HD ** (-0.5)
    query_pos = jnp.arange(WINDOW)[:, None] + WINDOW
    key_pos = jnp.arange(2 * WINDOW)[None, :]
    in_band = (key_pos <= query_pos) & (key_pos > query_pos - WINDOW)
    absolute = (
        lax.axis_index("sp") * seq_rows
        + jnp.arange(num_blocks)[:, None, None] * WINDOW
        + key_pos[None]
        - WINDOW
    )
    allowed = in_band[None] & (absolute >= 0)
    scores = jnp.where(allowed[:, None], scores, -jnp.inf)
    sink_col = jnp.broadcast_to(sink_logits[None, :, None, None], scores.shape[:-1] + (1,))
    combined = jnp.concatenate([scores, sink_col], axis=-1)
    row_max = jnp.max(combined, axis=-1, keepdims=True)
    exps = jnp.exp(combined - row_max)
    weights = (exps[..., :-1] / jnp.sum(exps, axis=-1, keepdims=True)).astype(jnp.bfloat16)
    attended = jnp.einsum("nhqs,nsd->nqhd", weights, values_ext, preferred_element_type=jnp.float32)
    return attended.astype(jnp.bfloat16).reshape(seq_rows, local_heads * HD)


def relative(x, axis):
    tp_count = lax.axis_size("tp")
    chips = tp_count // 2
    index = lax.axis_index("tp")
    shape = x.shape
    rows = shape[axis] // tp_count
    head, tail = shape[:axis], shape[axis + 1 :]
    x = x.reshape(head + (chips, 2, rows) + tail)
    bit = 1
    while bit < chips:
        y = x.reshape(head + (chips // (2 * bit), 2, bit, 2, rows) + tail)
        y = jnp.flip(y, len(head) + 1).reshape(x.shape)
        x = jnp.where(index // (2 * bit) % 2 == 1, y, x)
        bit = 2 * bit
    x = jnp.where(index % 2 == 1, jnp.flip(x, len(head) + 1), x)
    return jnp.swapaxes(x, len(head), len(head) + 1).reshape(shape)


def routing(expert_ids, expert_weights, expert_count, half_cap, lanes):
    seq_rows = expert_ids.shape[0]
    sp_count = lax.axis_size("sp")
    ids_t = expert_ids.T
    experts = jnp.arange(expert_count, dtype=jnp.int32)[:, None]
    named = jnp.zeros((expert_count, seq_rows), jnp.bool_)
    for k in range(TOPK):
        named = named | (ids_t[k : k + 1] == experts)
    row = lax.broadcasted_iota(jnp.int32, (seq_rows, seq_rows), 0)
    col = lax.broadcasted_iota(jnp.int32, (seq_rows, seq_rows), 1)
    before = (row < col).astype(jnp.bfloat16)
    earlier = dot(named.astype(jnp.bfloat16), before)
    tp_index = lax.axis_index("tp")
    spots = []
    for k in range(TOPK):
        ids_k = ids_t[k : k + 1]
        rank = jnp.sum(jnp.where(ids_k == experts, earlier, 0.0), axis=0, keepdims=True)
        rank = rank.astype(jnp.int32)
        here = (ids_k % lanes == tp_index // 2) & (rank // half_cap == tp_index % 2)
        step = (ids_k // lanes) ^ lax.axis_index("sp")
        if sp_count > 2:
            turned = step - step % 4 + step % 2 * 2 + step // 2 % 2
            step = jnp.where(tp_index % 2 == 1, turned, step)
        spots.append(jnp.where(here, step * half_cap + rank % half_cap, -1).astype(jnp.float32))
    table = relative(jnp.concatenate(spots + [expert_weights.T], axis=0), 1)
    slots = sp_count * half_cap

    def kernel(table_r, turned_r, pick_o, mix_o):
        def pick_block(i, carry):
            at = pl.ds(pl.multiple_of(i * 128, 128), 128)
            slot = lax.broadcasted_iota(jnp.int32, (128, seq_rows), 0) + i * 128
            hit = jnp.zeros((128, seq_rows), jnp.float32)
            for k in range(TOPK):
                spot = table_r[k : k + 1].astype(jnp.int32)
                hit = jnp.where(spot == slot, 1.0, hit)
            pick_o[at] = hit.astype(jnp.bfloat16)
            return carry

        def mix_block(i, carry):
            at = pl.ds(pl.multiple_of(i * 128, 128), 128)
            slot = lax.broadcasted_iota(jnp.int32, (128, slots), 1)
            mine = turned_r[at]
            mix = jnp.zeros((128, slots), jnp.float32)
            for k in range(TOPK):
                spot = mine[:, k : k + 1].astype(jnp.int32)
                mix = jnp.where(spot == slot, mine[:, TOPK + k : TOPK + k + 1], mix)
            mix_o[at] = mix.astype(jnp.bfloat16)
            return carry

        lax.fori_loop(0, slots // 128, pick_block, 0)
        lax.fori_loop(0, seq_rows // 128, mix_block, 0)

    return pl.pallas_call(
        kernel,
        out_shape=[
            jax.ShapeDtypeStruct((slots, seq_rows), jnp.bfloat16),
            jax.ShapeDtypeStruct((seq_rows, slots), jnp.bfloat16),
        ],
        in_specs=[WHOLE] * 2,
        out_specs=[WHOLE] * 2,
        compiler_params=ROOMY,
        name="matrices",
    )(table, table.T)


def dot_t(x, w):
    return lax.dot_general(x, w, (((1,), (1,)), ((), ())), preferred_element_type=jnp.float32)


def dot(x, w):
    return jnp.dot(x, w, preferred_element_type=jnp.float32)


def expert(sources, weights):
    units, width = weights[0][0].shape
    count, chunks = len(sources), len(sources[0])
    rows, part = sources[0][0].shape
    tile = min(256, units)
    tiles = units // tile
    out_tile = min(512, part)
    out_tiles = width // out_tile
    halves = len(weights)
    blocks = count * chunks

    def kernel(*refs):
        xs = refs[:blocks]
        ws = [refs[blocks + 3 * h : blocks + 3 * h + 3] for h in range(halves)]
        outs = refs[blocks + 3 * halves : 2 * blocks + 3 * halves]
        x_v, gate_v, up_v, down_v, hidden_v = refs[2 * blocks + 3 * halves : -3]
        x_sems, in_sems, out_sems = refs[-3:]
        loads = [
            pltpu.make_async_copy(
                xs[i * chunks + c],
                x_v.at[pl.ds(i * rows, rows), pl.ds(c * part, part)],
                x_sems.at[i, c],
            )
            for i in range(count)
            for c in range(chunks)
        ]
        pieces = [(0, 0, 1), (0, 1, tiles)] if tiles > 1 else [(0, 0, tiles)]
        pieces = pieces + [(h, 0, tiles) for h in range(1, halves)]
        queue = []
        for i, (h, low, high) in enumerate(pieces):
            at = pl.ds(low * tile, (high - low) * tile)
            into = pl.ds(h * units + low * tile, (high - low) * tile)
            queue.append(
                [
                    pltpu.make_async_copy(ws[h][0].at[at], gate_v.at[into], in_sems.at[i, 0]),
                    pltpu.make_async_copy(ws[h][1].at[at], up_v.at[into], in_sems.at[i, 1]),
                ]
            )
        for c in range(chunks):
            at = pl.ds(c * part, part)
            queue.append(
                [
                    pltpu.make_async_copy(
                        ws[h][2].at[:, at], down_v.at[pl.ds(h * units, units), at], out_sems.at[c, h]
                    )
                    for h in range(halves)
                ]
            )

        def ready(i):
            for copy in queue[i + AHEAD] if i + AHEAD < len(queue) else ():
                copy.start()
            for copy in queue[i]:
                copy.wait()

        for pair in [loads] + queue[:AHEAD]:
            for copy in pair:
                copy.start()
        for copy in loads:
            copy.wait()
        starts = [h * tiles + low for h, low, _ in pieces]
        for i in range(halves * tiles):
            if i in starts:
                ready(starts.index(i))
            at = pl.ds(i * tile, tile)
            gate = dot_t(x_v[...], gate_v[at])
            up = dot_t(x_v[...], up_v[at])
            hidden_v[:, at] = (gate / (1.0 + jnp.exp(-gate)) * up).astype(jnp.bfloat16)
        for t in range(out_tiles):
            col = t * out_tile
            if col % part == 0:
                ready(len(pieces) + col // part)
            out = dot(hidden_v[...], down_v[:, pl.ds(col, out_tile)]).astype(jnp.bfloat16)
            for i in range(count):
                outs[i * chunks + col // part][:, pl.ds(col % part, out_tile)] = out[
                    i * rows : (i + 1) * rows
                ]

    raw = pl.BlockSpec(memory_space=pl.ANY)
    all_rows = count * rows
    outs = pl.pallas_call(
        kernel,
        out_shape=[jax.ShapeDtypeStruct((rows, part), jnp.bfloat16)] * blocks,
        in_specs=[raw] * (blocks + 3 * halves),
        out_specs=[WHOLE] * blocks,
        scratch_shapes=[
            pltpu.VMEM((all_rows, width), jnp.bfloat16),
            pltpu.VMEM((halves * units, width), jnp.bfloat16),
            pltpu.VMEM((halves * units, width), jnp.bfloat16),
            pltpu.VMEM((halves * units, width), jnp.bfloat16),
            pltpu.VMEM((all_rows, halves * units), jnp.bfloat16),
            pltpu.SemaphoreType.DMA((count, chunks)),
            pltpu.SemaphoreType.DMA((halves + 1, 2)),
            pltpu.SemaphoreType.DMA((chunks, halves)),
        ],
        compiler_params=ROOMY,
        cost_estimate=pl.CostEstimate(
            flops=6 * all_rows * halves * units * width,
            bytes_accessed=6 * halves * units * width + 4 * all_rows * width,
            transcendentals=all_rows * halves * units,
        ),
        name="expert",
    )(*[x for source in sources for x in source], *[w for half in weights for w in half])
    return [outs[i * chunks : (i + 1) * chunks] for i in range(count)]


def slot_capacity(seq_rows, sp_count, tp_count):
    return max(2, 2 * seq_rows * TOPK // (sp_count * tp_count // 2))


def source_groups(sp_count, half_cap):
    size = max(1, 256 // half_cap)
    steps = list(range(1, sp_count))
    return [[0]] + [steps[i : i + size] for i in range(0, len(steps), size)]


def project(heads, w_near, w_far, residual, norm_gain, chunks):
    rows, width = residual.shape
    count, steps = len(heads), len(w_far)
    part = width // chunks
    cols = heads[0].shape[1] // 2
    share = width // steps

    def kernel(index, *refs):
        att, near = refs[:count], refs[count : count + 2]
        far = refs[count + 2 : count + 2 + 2 * steps]
        res, gain, mixed = refs[count + 2 + 2 * steps : count + 5 + 2 * steps]
        outs, total_v = refs[count + 5 + 2 * steps : -1], refs[-1]
        total = res[...].astype(jnp.float32)
        for h in range(2):
            total = total + dot(att[0][:, h * cols : (h + 1) * cols], near[h][...])
        total_v[...] = total
        sides = [
            jnp.concatenate([att[k][:, h * cols : (h + 1) * cols] for k in range(1, count)], axis=1)
            for h in range(2)
        ]
        for step in range(steps):
            at = pl.ds(pl.multiple_of((index[0] ^ step) * share, share), share)
            for h in range(2):
                total_v[:, at] = total_v[:, at] + dot(sides[h], far[2 * step + h][...])
        after = total_v[...].astype(jnp.bfloat16)
        mixed[...] = after
        after = after.astype(jnp.float32)
        scale = lax.rsqrt(jnp.mean(after * after, axis=-1, keepdims=True) + 1e-06)
        normed = (after * scale * gain[...]).astype(jnp.bfloat16)
        for c in range(chunks):
            outs[c][...] = normed[:, c * part : (c + 1) * part]

    index = lax.axis_index("sp").astype(jnp.int32)[None]
    return pl.pallas_call(
        kernel,
        out_shape=[jax.ShapeDtypeStruct((rows, width), jnp.bfloat16)]
        + [jax.ShapeDtypeStruct((rows, part), jnp.bfloat16)] * chunks,
        in_specs=[pl.BlockSpec(memory_space=pltpu.SMEM)] + [WHOLE] * (count + 4 + 2 * steps),
        out_specs=[WHOLE] * (chunks + 1),
        scratch_shapes=[pltpu.VMEM((rows, width), jnp.float32)],
        compiler_params=ROOMY,
        name="project",
    )(index, *heads, *w_near, *[x for pair in w_far for x in pair], residual, norm_gain[None])


def pick_rows(pick, blocks, gate, up, sp_count):
    seq_rows = pick.shape[1]
    half_cap = pick.shape[0] // sp_count
    rows, part = blocks[0].shape
    units = gate.shape[0]
    count = len(blocks)

    def kernel(*refs):
        pick_r, parts = refs[0], refs[1 : 1 + count]
        gate_r, up_r = refs[1 + count : 3 + count]
        outs = refs[3 + count : 3 + count + sp_count]
        gate_o, up_o, rows_v = refs[3 + count + sp_count :]
        for i in range(count):
            rows_v[i * rows : (i + 1) * rows] = parts[i][...]

        def columns(t, carry):
            at = pl.ds(pl.multiple_of(t * 256, 256), 256)
            for step in range(sp_count):
                slots = pl.ds(step * half_cap, half_cap)
                outs[step][:, at] = dot(pick_r[slots], rows_v[:, at]).astype(jnp.bfloat16)
            return carry

        lax.fori_loop(0, part // 256, columns, 0)
        gate_o[...] = dot_t(rows_v[...], gate_r[...])
        up_o[...] = dot_t(rows_v[...], up_r[...])

    return pl.pallas_call(
        kernel,
        out_shape=[jax.ShapeDtypeStruct((half_cap, part), jnp.bfloat16)] * sp_count
        + [jax.ShapeDtypeStruct((seq_rows, units), jnp.float32)] * 2,
        in_specs=[WHOLE] * (3 + count),
        out_specs=[WHOLE] * (2 + sp_count),
        scratch_shapes=[pltpu.VMEM((seq_rows, part), jnp.bfloat16)],
        compiler_params=ROOMY,
        name="pick_rows",
    )(pick, *blocks, gate, up)


def combine(mix, held, hidden, down, half, arrived):
    rows = mix.shape[0] // 2
    sp_count = len(held)
    half_cap, part = held[0].shape
    chips = lax.axis_size("tp") // 2
    outs_n = 1 if arrived is None else chips

    def kernel(*refs):
        mix_r, parts, hid, down_r = refs[0], refs[1 : 1 + sp_count], *refs[1 + sp_count : 3 + sp_count]
        outs = refs[-outs_n - 1 : -1]
        held_v = refs[-1]
        for step in range(sp_count):
            held_v[step * half_cap : (step + 1) * half_cap] = parts[step][...]
        each = rows // outs_n

        def columns(t, carry):
            at = pl.ds(pl.multiple_of(t * 512, 512), 512)
            total = dot(mix_r[...], held_v[:, at]) + dot(hid[...], down_r[:, at])
            if arrived is not None:
                total = total + refs[3 + sp_count][:, at].astype(jnp.float32)
            total = total.astype(jnp.bfloat16)
            for i in range(outs_n):
                outs[i][:, at] = total[i * each : (i + 1) * each]
            return carry

        lax.fori_loop(0, part // 512, columns, 0)

    def block(x):
        return pl.BlockSpec((rows, x.shape[1]), lambda i: (half, 0))

    full = lambda x: pl.BlockSpec(x.shape, lambda i: (0, 0))
    more = [] if arrived is None else [arrived]
    return pl.pallas_call(
        kernel,
        grid=(1,),
        out_shape=[jax.ShapeDtypeStruct((rows // outs_n, part), jnp.bfloat16)] * outs_n,
        in_specs=[block(mix)]
        + [full(x) for x in held]
        + [block(hidden), full(down)]
        + [full(x) for x in more],
        out_specs=[pl.BlockSpec((rows // outs_n, part), lambda i: (0, 0))] * outs_n,
        scratch_shapes=[pltpu.VMEM((sp_count * half_cap, part), jnp.bfloat16)],
        compiler_params=ROOMY,
        name="combine",
    )(mix, *held, hidden, down, *more)


def crossing(step, core):
    return (step - step % 4) + (0, 2, 1, 3)[step % 4] if core else step


def cross(x, step):
    if step == 0:
        return x
    sp_count, tp_count = lax.axis_size("sp"), lax.axis_size("tp")
    route = [
        (i * tp_count + t, (i ^ (crossing(step, t % 2) if sp_count > 2 else step)) * tp_count + t)
        for i in range(sp_count)
        for t in range(tp_count)
    ]
    return lax.ppermute(x, ("sp", "tp"), route)


def high_bits(count):
    return [1 << b for b in reversed(range(count.bit_length() - 1))]


def body(
    queries,
    keys,
    values,
    sink_logits,
    w_out,
    residual,
    norm_gain,
    expert_ids,
    expert_weights,
    w_gate,
    w_up,
    w_down,
    shared_gate,
    shared_up,
    shared_down,
):
    tp_count = lax.axis_size("tp")
    sp_count = lax.axis_size("sp")
    seq_rows = queries.shape[0]
    width = residual.shape[1]
    expert_count = sp_count * tp_count // 2
    half_cap = slot_capacity(seq_rows, sp_count, tp_count) // 2
    lanes = tp_count // 2
    chips = tp_count // 2
    share = width // sp_count
    own_share = lax.dynamic_slice_in_dim(w_out, lax.axis_index("sp") * share, share, 1)
    column = [own_share] + [None] * (chips - 1)
    for bit in high_bits(chips):
        for k in range(0, chips, 2 * bit):
            if column[k] is not None:
                column[k | bit] = peer(column[k], "tp", 2 * bit)
    column = jnp.concatenate(column[1:], axis=0)
    shares = [peer(column, "sp", step) for step in range(sp_count)]
    w_far = [(x, peer(x, "tp", 1)) for x in shares]
    w_near = (w_out, peer(w_out, "tp", 1))
    gates = (w_gate[0], peer(w_gate[0], "tp", 1))
    ups = (w_up[0], peer(w_up[0], "tp", 1))
    downs = (w_down[0], peer(w_down[0], "tp", 1))
    attended = relative(attention(queries, keys, values, sink_logits), 0)
    half_rows = seq_rows // 2
    others = peer(attended[half_rows:], "tp", 1)
    both = jnp.concatenate([attended[:half_rows], others], axis=1)
    own_rows = residual.shape[0]
    heads = [peer(both[k * own_rows : (k + 1) * own_rows], "tp", 2 * k) for k in range(chips)]
    after_mix, *normed = project(heads, w_near, w_far, residual, norm_gain, CHUNKS)
    pick, mix = routing(expert_ids, expert_weights, expert_count, half_cap, lanes)
    cuts = [slice(c * width // CHUNKS, (c + 1) * width // CHUNKS) for c in range(CHUNKS)]
    arrived = [[None] * CHUNKS for _ in range(sp_count)]
    shared_g, shared_u = 0.0, 0.0
    for c in range(CHUNKS):
        mine = [normed[c]] + [None] * (chips - 1)
        for bit in high_bits(chips):
            for k in range(chips):
                if mine[k] is not None and k & bit == 0 and k % (2 * bit) == 0:
                    mine[k | bit] = peer(mine[k], "tp", 2 * bit)
        theirs = [peer(mine[k], "tp", 1) for k in range(chips)]
        *picked, gate_part, up_part = pick_rows(
            pick, mine + theirs, shared_gate[:, cuts[c]], shared_up[:, cuts[c]], sp_count
        )
        shared_g, shared_u = shared_g + gate_part, shared_u + up_part
        for step in range(sp_count):
            arrived[step][c] = cross(picked[step], step)
    shared_hidden = (jax.nn.silu(shared_g) * shared_u).astype(jnp.bfloat16)
    weights = tuple(zip(gates, ups, downs))
    held = []
    for group in source_groups(sp_count, half_cap):
        outs = expert([arrived[step] for step in group], weights)
        for step, parts in zip(group, outs):
            held.append([cross(parts[c], step) for c in range(CHUNKS)])
    results = []
    for c in range(CHUNKS):
        back = [held[step][c] for step in range(sp_count)]
        down = shared_down[:, cuts[c]]
        (for_mate,) = combine(mix, back, shared_hidden, down, 1, None)
        from_mate = peer(for_mate, "tp", 1)
        sums = combine(mix, back, shared_hidden, down, 0, from_mate)
        sums = [x.astype(jnp.float32) for x in sums]
        sums[0] = sums[0] + after_mix[:, cuts[c]].astype(jnp.float32)
        for bit in reversed(high_bits(chips)):
            for k in range(0, chips, 2 * bit):
                sent = peer(sums[k | bit].astype(jnp.bfloat16), "tp", 2 * bit)
                sums[k] = sums[k] + sent.astype(jnp.float32)
        results.append(sums[0].astype(jnp.bfloat16))
    return jnp.concatenate(results, axis=1)


def solution(mesh):
    return jax.shard_map(
        body,
        mesh=mesh,
        in_specs=(
            P("sp", "tp"),
            P("sp", None),
            P("sp", None),
            P("tp"),
            P("tp", None),
            P(("sp", "tp"), None),
            P(),
            P("sp", None),
            P("sp", None),
            P(("sp", "tp"), None, None),
            P(("sp", "tp"), None, None),
            P(("sp", "tp"), None, None),
            P("tp", None),
            P("tp", None),
            P("tp", None),
        ),
        out_specs=P(("sp", "tp"), None),
        check_vma=False,
    )
```

profile of v0, /device:TPU:0, one launch (start us, length us, event | category | flops | bytes accessed | tf_op | source)
XLA Modules:
  0.0 264.7 jit_solution(8572882723958368152)
XLA Ops:
  0.0 1.6 constant_dynamic-slice_fusion
  1.6 4.1 %collective-permute-start.7 = (bf16[128,512]{1,0:T(8,128)(2,1)}, bf16[128,512]{1,0:T(8,128)(2,1)S(1)}, u32[]{:S(2)}, u32[]{:S(2)}) collective-permute-start(bf16[128,512]{1,0:T(8,128)(2,1)} %constant_dynamic-slice_fusion), channel_id=1, source_target_pairs={{0,4},{1,5},{2,6},{3,7},{4,0},{5,1},{6,2},{7,3},{8,12},{9,13},{10,... | collective-permute-start | bytes 393224 | tf_op jit(solution)/shard_map/ppermute | solution.py:30
  5.7 1.6 collective-permute-start.6
  7.3 1.2 constant_dynamic-slice_fusion.1
  8.8 3.4 %collective-permute-start = (bf16[128,128]{0,1:T(8,128)(2,1)S(1)}, bf16[128,128]{0,1:T(8,128)(2,1)S(1)}, u32[]{:S(2)}, u32[]{:S(2)}) collective-permute-start(bf16[128,128]{0,1:T(8,128)(2,1)S(1)} %pad_maximum_fusion.2), channel_id=1, source_target_pairs={{0,8},{8,16},{16,24},{1,9},{9,17},{17,25},{2,10},{10,18},{18,26},{... | collective-permute-start | bytes 98312 | tf_op jit(solution)/shard_map/ppermute | solution.py:23
  16.8 1.9 copy.42
  19.6 1.1 select_select_fusion.1
  22.3 4.4 %collective-permute-done.8 = bf16[128,512]{1,0:T(8,128)(2,1)S(1)} collective-permute-done((bf16[128,512]{1,0:T(8,128)(2,1)S(1)}, bf16[128,512]{1,0:T(8,128)(2,1)S(1)}, u32[]{:S(2)}, u32[]{:S(2)}) %collective-permute-start.8) | collective-permute-done | bytes 131104 | tf_op jit(solution)/shard_map/ppermute | solution.py:30
  26.8 2.4 collective-permute-start.10
  29.2 1.5 collective-permute-start.12
  32.1 3.8 %collective-permute-done.2.refs_1_ = bf16[128,256]{1,0:T(8,128)(2,1)S(1)} collective-permute-done((bf16[128,256]{1,0:T(8,128)(2,1)S(1)}, bf16[128,256]{1,0:T(8,128)(2,1)S(1)}, u32[]{:S(2)}, u32[]{:S(2)}) %collective-permute-start.2) | collective-permute-done | bytes 65568 | tf_op jit(solution)/shard_map/ppermute | solution.py:30
  36.3 6.0 %collective-permute-done.3.refs_2_ = bf16[128,256]{1,0:T(8,128)(2,1)S(1)} collective-permute-done((bf16[128,256]{1,0:T(8,128)(2,1)S(1)}, bf16[128,256]{1,0:T(8,128)(2,1)S(1)}, u32[]{:S(2)}, u32[]{:S(2)}) %collective-permute-start.3) | collective-permute-done | bytes 65568 | tf_op jit(solution)/shard_map/ppermute | solution.py:30
  42.4 6.1 %collective-permute-done.4.refs_3_ = bf16[128,256]{1,0:T(8,128)(2,1)S(1)} collective-permute-done((bf16[128,256]{1,0:T(8,128)(2,1)S(1)}, bf16[128,256]{1,0:T(8,128)(2,1)S(1)}, u32[]{:S(2)}, u32[]{:S(2)}) %collective-permute-start.4) | collective-permute-done | bytes 65568 | tf_op jit(solution)/shard_map/ppermute | solution.py:30
  51.9 1.2 project.1
  54.5 12.8 %collective-permute-done.24.refs_3_ = bf16[128,1024]{1,0:T(8,128)(2,1)} collective-permute-done((bf16[128,1024]{1,0:T(8,128)(2,1)S(1)}, bf16[128,1024]{1,0:T(8,128)(2,1)}, u32[]{:S(2)}, u32[]{:S(2)}) %collective-permute-start.24) | collective-permute-done | bytes 262176 | tf_op jit(solution)/shard_map/ppermute | solution.py:30
  69.5 1.4 collective-permute-start.16
  71.0 11.5 %collective-permute-done.17.refs_3_ = bf16[128,1024]{1,0:T(8,128)(2,1)} collective-permute-done((bf16[128,1024]{1,0:T(8,128)(2,1)S(1)}, bf16[128,1024]{1,0:T(8,128)(2,1)}, u32[]{:S(2)}, u32[]{:S(2)}) %collective-permute-start.17) | collective-permute-done | bytes 262176 | tf_op jit(solution)/shard_map/ppermute | solution.py:30
  82.5 1.0 collective-permute-done.16.refs_2_
  86.1 5.4 %collective-permute-done.25.refs_4_ = bf16[128,1024]{1,0:T(8,128)(2,1)S(1)} collective-permute-done((bf16[128,1024]{1,0:T(8,128)(2,1)}, bf16[128,1024]{1,0:T(8,128)(2,1)S(1)}, u32[]{:S(2)}, u32[]{:S(2)}) %collective-permute-start.25) | collective-permute-done | bytes 262176 | tf_op jit(solution)/shard_map/ppermute | solution.py:30
  93.7 1.0 copy.28
  94.7 1.0 copy.29
  95.7 1.0 copy.30
  96.7 4.5 %collective-permute-done.18.refs_4_ = bf16[128,1024]{1,0:T(8,128)(2,1)} collective-permute-done((bf16[128,1024]{1,0:T(8,128)(2,1)}, bf16[128,1024]{1,0:T(8,128)(2,1)}, u32[]{:S(2)}, u32[]{:S(2)}) %collective-permute-start.18) | collective-permute-done | bytes 262176 | tf_op jit(solution)/shard_map/ppermute | solution.py:30
  101.2 1.1 select_select_fusion
  105.1 1.2 copy.31.table_r
  106.3 1.1 copy-done.2
  107.3 4.6 %matrices.1 = (bf16[1024,1024]{1,0:T(8,128)(2,1)S(1)}, bf16[1024,1024]{1,0:T(8,128)(2,1)S(1)}) custom-call(f32[8,1024]{1,0:T(8,128)S(1)} %copy.31.table_r, f32[1024,8]{1,0:T(8,128)S(1)} %bitcast.91), custom_call_target="tpu_custom_call" | custom-call | tf_op jit(solution)/shard_map/matrices/pallas_call | solution.py:147
  111.9 1.1 fusion.58
  114.0 0.9 copy-done.12
  115.0 0.9 copy-done.16
  116.9 0.9 copy-done.20
  118.8 5.3 %pick_rows.3 = (bf16[256,1024]{1,0:T(8,128)(2,1)S(1)}, bf16[256,1024]{1,0:T(8,128)(2,1)S(1)}, bf16[256,1024]{1,0:T(8,128)(2,1)S(1)}, bf16[256,1024]{1,0:T(8,128)...) custom-call(bf16[1024,1024]{1,0:T(8,128)(2,1)S(1)} %get-tuple-element.39.refs_0_, ...), custom_call_target="tpu_custom_call" | custom-call | tf_op jit(solution)/shard_map/pick_rows/pallas_call | solution.py:355
  124.1 2.2 collective-permute-start.40
  126.4 5.6 %pick_rows.2 = (bf16[256,1024]{1,0:T(8,128)(2,1)S(1)}, bf16[256,1024]{1,0:T(8,128)(2,1)S(1)}, bf16[256,1024]{1,0:T(8,128)(2,1)S(1)}, bf16[256,1024]{1,0:T(8,128)...) custom-call(bf16[1024,1024]{1,0:T(8,128)(2,1)S(1)} %get-tuple-element.39.refs_0_, ...), custom_call_target="tpu_custom_call" | custom-call | tf_op jit(solution)/shard_map/pick_rows/pallas_call | solution.py:355
  132.8 7.1 %collective-permute-done.40.refs_1_ = bf16[256,1024]{1,0:T(8,128)(2,1)S(1)} collective-permute-done((bf16[256,1024]{1,0:T(8,128)(2,1)S(1)}, bf16[256,1024]{1,0:T(8,128)(2,1)S(1)}, u32[]{:S(2)}, u32[]{:S(2)}) %collective-permute-start.40) | collective-permute-done | bytes 524320 | tf_op jit(solution)/shard_map/ppermute | solution.py:427
  139.9 2.0 collective-permute-start.37
  141.9 9.3 %collective-permute-done.39.refs_0_ = bf16[256,1024]{1,0:T(8,128)(2,1)S(1)} collective-permute-done((bf16[256,1024]{1,0:T(8,128)(2,1)S(1)}, bf16[256,1024]{1,0:T(8,128)(2,1)S(1)}, u32[]{:S(2)}, u32[]{:S(2)}) %collective-permute-start.39) | collective-permute-done | bytes 524320 | tf_op jit(solution)/shard_map/ppermute | solution.py:427
  151.2 2.0 collective-permute-start.36
  154.0 1.4 collective-permute-start.33
  155.3 7.3 %expert.7 = (bf16[256,1024]{1,0:T(8,128)(2,1)S(1)}, bf16[256,1024]{1,0:T(8,128)(2,1)S(1)}) custom-call(bf16[256,1024]{1,0:T(8,128)(2,1)S(1)} %collective-permute-done.39.refs_0_, bf16[256,1024]{1,0:T(8,128)(2,1)S(1)} %collective-permute-done.40.refs_1_, bf16[768,2048]{1,0:T(8,128)(2,1)S(1)} %bitcast.81, bf16[768,2048]{1,0:T(8,128)(2,1)S(1)} %bitcast.86, ...), custom_call_target="tpu_custom_call" | custom-call | flops 4831838208 | bytes 20971520 | tf_op jit(solution)/shard_map/expert/pallas_call | solution.py:248
  163.2 9.1 %collective-permute-done.36.refs_0_ = bf16[256,1024]{1,0:T(8,128)(2,1)S(1)} collective-permute-done((bf16[256,1024]{1,0:T(8,128)(2,1)S(1)}, bf16[256,1024]{1,0:T(8,128)(2,1)S(1)}, u32[]{:S(2)}, u32[]{:S(2)}) %collective-permute-start.36) | collective-permute-done | bytes 524320 | tf_op jit(solution)/shard_map/ppermute | solution.py:427
  172.3 7.5 %expert.6 = (bf16[256,1024]{1,0:T(8,128)(2,1)S(1)}, bf16[256,1024]{1,0:T(8,128)(2,1)S(1)}) custom-call(bf16[256,1024]{1,0:T(8,128)(2,1)S(1)} %collective-permute-done.36.refs_0_, bf16[256,1024]{1,0:T(8,128)(2,1)S(1)} %collective-permute-done.37.refs_1_, bf16[768,2048]{1,0:T(8,128)(2,1)S(1)} %bitcast.82, bf16[768,2048]{1,0:T(8,128)(2,1)S(1)} %bitcast.87, ...), custom_call_target="tpu_custom_call" | custom-call | flops 4831838208 | bytes 20971520 | tf_op jit(solution)/shard_map/expert/pallas_call | solution.py:248
  179.8 2.9 %collective-permute-start.47 = (bf16[256,1024]{1,0:T(8,128)(2,1)S(1)}, bf16[256,1024]{1,0:T(8,128)(2,1)S(1)}, u32[]{:S(2)}, u32[]{:S(2)}) collective-permute-start(bf16[256,1024]{1,0:T(8,128)(2,1)S(1)} %get-tuple-element.65), channel_id=1, source_target_pairs={{0,16},{1,9},{2,18},{3,11},{4,20},{5,13},{6,22},{7,15},{8,24},{9,1... | collective-permute-start | bytes 1572872 | tf_op jit(solution)/shard_map/ppermute | solution.py:427
  182.7 7.3 %expert.5 = (bf16[256,1024]{1,0:T(8,128)(2,1)S(1)}, bf16[256,1024]{1,0:T(8,128)(2,1)S(1)}) custom-call(bf16[256,1024]{1,0:T(8,128)(2,1)S(1)} %collective-permute-done.33.refs_0_, bf16[256,1024]{1,0:T(8,128)(2,1)S(1)} %collective-permute-done.34.refs_1_, bf16[768,2048]{1,0:T(8,128)(2,1)S(1)} %bitcast.83, bf16[768,2048]{1,0:T(8,128)(2,1)S(1)} %bitcast.88, ...), custom_call_target="tpu_custom_call" | custom-call | flops 4831838208 | bytes 20971520 | tf_op jit(solution)/shard_map/expert/pallas_call | solution.py:248
  190.2 1.5 collective-permute-start.41
  191.8 2.0 collective-permute-start.38
  193.8 7.5 %expert.4 = (bf16[256,1024]{1,0:T(8,128)(2,1)S(1)}, bf16[256,1024]{1,0:T(8,128)(2,1)S(1)}) custom-call(bf16[256,1024]{1,0:T(8,128)(2,1)S(1)} %get-tuple-element.41.refs_0_, bf16[256,1024]{1,0:T(8,128)(2,1)S(1)} %get-tuple-element.43.refs_1_, bf16[768,2048]{1,0:T(8,128)(2,1)S(1)} %bitcast.84, bf16[768,2048]{1,0:T(8,128)(2,1)S(1)} %bitcast.89, ...), custom_call_target="tpu_custom_call" | custom-call | flops 4831838208 | bytes 20971520 | tf_op jit(solution)/shard_map/expert/pallas_call | solution.py:248
  201.7 3.1 %collective-permute-done.46.refs_2_ = bf16[256,1024]{1,0:T(8,128)(2,1)S(1)} collective-permute-done((bf16[256,1024]{1,0:T(8,128)(2,1)S(1)}, bf16[256,1024]{1,0:T(8,128)(2,1)S(1)}, u32[]{:S(2)}, u32[]{:S(2)}) %collective-permute-start.46) | collective-permute-done | bytes 524320 | tf_op jit(solution)/shard_map/ppermute | solution.py:427
  204.8 1.8 combine.6
  206.6 3.5 %collective-permute-start.49 = (bf16[512,1024]{1,0:T(8,128)(2,1)S(1)}, bf16[512,1024]{1,0:T(8,128)(2,1)S(1)}, u32[]{:S(2)}, u32[]{:S(2)}) collective-permute-start(bf16[512,1024]{1,0:T(8,128)(2,1)S(1)} %combine.6), channel_id=1, source_target_pairs={{0,1},{1,0},{2,3},{3,2},{4,5},{5,4},{6,7},{7,6},{8,9},{9,8},{10,11... | collective-permute-start | bytes 3145736 | tf_op jit(solution)/shard_map/ppermute | solution.py:30
  210.1 3.8 %collective-permute-done.41.refs_4_ = bf16[256,1024]{1,0:T(8,128)(2,1)S(1)} collective-permute-done((bf16[256,1024]{1,0:T(8,128)(2,1)S(1)}, bf16[256,1024]{1,0:T(8,128)(2,1)S(1)}, u32[]{:S(2)}, u32[]{:S(2)}) %collective-permute-start.41) | collective-permute-done | bytes 524320 | tf_op jit(solution)/shard_map/ppermute | solution.py:427
  213.9 4.6 %collective-permute-done.38.refs_3_ = bf16[256,1024]{1,0:T(8,128)(2,1)S(1)} collective-permute-done((bf16[256,1024]{1,0:T(8,128)(2,1)S(1)}, bf16[256,1024]{1,0:T(8,128)(2,1)S(1)}, u32[]{:S(2)}, u32[]{:S(2)}) %collective-permute-start.38) | collective-permute-done | bytes 524320 | tf_op jit(solution)/shard_map/ppermute | solution.py:427
  218.8 1.8 combine.4
  220.6 1.9 collective-permute-start.42
  222.5 1.8 combine.7
  224.8 1.8 combine.5
  226.6 1.7 collective-permute-start.44
  228.7 1.6 collective-permute-start.43
  230.3 3.3 %collective-permute-done.51 = bf16[128,1024]{1,0:T(8,128)(2,1)S(1)} collective-permute-done((bf16[128,1024]{1,0:T(8,128)(2,1)S(1)}, bf16[128,1024]{1,0:T(8,128)(2,1)S(1)}, u32[]{:S(2)}, u32[]{:S(2)}) %collective-permute-start.51) | collective-permute-done | bytes 262176 | tf_op jit(solution)/shard_map/ppermute | solution.py:30
  234.3 10.5 %collective-permute-done.44 = bf16[128,1024]{1,0:T(8,128)(2,1)S(1)} collective-permute-done((bf16[128,1024]{1,0:T(8,128)(2,1)S(1)}, bf16[128,1024]{1,0:T(8,128)(2,1)S(1)}, u32[]{:S(2)}, u32[]{:S(2)}) %collective-permute-start.44) | collective-permute-done | bytes 262176 | tf_op jit(solution)/shard_map/ppermute | solution.py:30
  244.9 8.4 %collective-permute-done.50 = bf16[128,1024]{1,0:T(8,128)(2,1)S(1)} collective-permute-done((bf16[128,1024]{1,0:T(8,128)(2,1)S(1)}, bf16[128,1024]{1,0:T(8,128)(2,1)S(1)}, u32[]{:S(2)}, u32[]{:S(2)}) %collective-permute-start.50) | collective-permute-done | bytes 262176 | tf_op jit(solution)/shard_map/ppermute | solution.py:30
  253.3 4.7 %collective-permute-done.43 = bf16[128,1024]{1,0:T(8,128)(2,1)S(1)} collective-permute-done((bf16[128,1024]{1,0:T(8,128)(2,1)S(1)}, bf16[128,1024]{1,0:T(8,128)(2,1)S(1)}, u32[]{:S(2)}, u32[]{:S(2)}) %collective-permute-start.43) | collective-permute-done | bytes 262176 | tf_op jit(solution)/shard_map/ppermute | solution.py:30
  258.0 5.5 %collective-permute-done.45 = bf16[128,1024]{1,0:T(8,128)(2,1)S(1)} collective-permute-done((bf16[128,1024]{1,0:T(8,128)(2,1)S(1)}, bf16[128,1024]{1,0:T(8,128)(2,1)S(1)}, u32[]{:S(2)}, u32[]{:S(2)}) %collective-permute-start.45) | collective-permute-done | bytes 262176 | tf_op jit(solution)/shard_map/ppermute | solution.py:30
  263.5 1.1 add_convert_fusion.2
  (176 shorter events, 31.3 us)
Async XLA Ops:
  0.0 12.9 %copy-start.26 = (bf16[1024,128]{1,0:T(8,128)(2,1)S(1)}, bf16[1024,128]{1,0:T(8,128)(2,1)}, u32[]{:S(2)}) copy-start(bf16[1024,128]{1,0:T(8,128)(2,1)} %param.15) | copy-start | bytes 786436
  1.6 19.3 %collective-permute-start.7 = (bf16[128,512]{1,0:T(8,128)(2,1)}, bf16[128,512]{1,0:T(8,128)(2,1)S(1)}, u32[]{:S(2)}, u32[]{:S(2)}) collective-permute-start(bf16[128,512]{1,0:T(8,128)(2,1)} %constant_dynamic-slice_fusion), channel_id=1, source_target_pairs={{0,4},{1,5},{2,6},{3,7},{4,0},{5,1},{6,2},{7,3},{8,12},{9,13},{10,... | collective-permute-start | bytes 393224 | tf_op jit(solution)/shard_map/ppermute | solution.py:30
  5.7 15.7 %collective-permute-start.6 = (bf16[128,512]{1,0:T(8,128)(2,1)}, bf16[128,512]{1,0:T(8,128)(2,1)}, u32[]{:S(2)}, u32[]{:S(2)}) collective-permute-start(bf16[128,512]{1,0:T(8,128)(2,1)} %constant_dynamic-slice_fusion), channel_id=1, source_target_pairs={{0,2},{1,3},{2,0},{3,1},{4,6},{5,7},{6,4},{7,5},{8,10},{9,11},{10,... | collective-permute-start | bytes 393224 | tf_op jit(solution)/shard_map/ppermute | solution.py:30
  8.8 5.0 %collective-permute-start = (bf16[128,128]{0,1:T(8,128)(2,1)S(1)}, bf16[128,128]{0,1:T(8,128)(2,1)S(1)}, u32[]{:S(2)}, u32[]{:S(2)}) collective-permute-start(bf16[128,128]{0,1:T(8,128)(2,1)S(1)} %pad_maximum_fusion.2), channel_id=1, source_target_pairs={{0,8},{8,16},{16,24},{1,9},{9,17},{17,25},{2,10},{10,18},{18,26},{... | collective-permute-start | bytes 98312 | tf_op jit(solution)/shard_map/ppermute | solution.py:23
  16.8 32.6 %copy-start = (bf16[1,768,2048]{2,1,0:T(8,128)(2,1)S(1)}, bf16[1,768,2048]{2,1,0:T(8,128)(2,1)}, u32[]{:S(2)}) copy-start(bf16[1,768,2048]{2,1,0:T(8,128)(2,1)} %param.24) | copy-start | bytes 9437188
  16.8 35.0 %copy-start.25 = (f32[2048]{0:T(1024)S(1)}, f32[2048]{0:T(1024)}, u32[]{:S(2)}) copy-start(f32[2048]{0:T(1024)} %param.21) | copy-start | bytes 24580
  19.6 12.5 %copy-start.3 = (bf16[128,2048]{1,0:T(8,128)(2,1)S(1)}, bf16[128,2048]{1,0:T(8,128)(2,1)}, u32[]{:S(2)}) copy-start(bf16[128,2048]{1,0:T(8,128)(2,1)} %refs_4_.1) | copy-start | bytes 1572868
  19.6 32.2 %copy-start.4 = (bf16[128,2048]{1,0:T(8,128)(2,1)S(1)}, bf16[128,2048]{1,0:T(8,128)(2,1)}, u32[]{:S(2)}) copy-start(bf16[128,2048]{1,0:T(8,128)(2,1)} %refs_14_.1) | copy-start | bytes 1572868
  20.8 10.8 %collective-permute-start.1 = (bf16[512,128]{1,0:T(8,128)(2,1)S(1)}, bf16[512,128]{1,0:T(8,128)(2,1)S(1)}, u32[]{:S(2)}, u32[]{:S(2)}) collective-permute-start(bf16[512,128]{1,0:T(8,128)(2,1)S(1)} %bitcast.106), channel_id=1, source_target_pairs={{0,1},{1,0},{2,3},{3,2},{4,5},{5,4},{6,7},{7,6},{8,9},{9,8},{10,11... | collective-permute-start | bytes 393224 | tf_op jit(solution)/shard_map/ppermute | solution.py:30
  20.9 5.9 %collective-permute-start.8 = (bf16[128,512]{1,0:T(8,128)(2,1)S(1)}, bf16[128,512]{1,0:T(8,128)(2,1)S(1)}, u32[]{:S(2)}, u32[]{:S(2)}) collective-permute-start(bf16[128,512]{1,0:T(8,128)(2,1)S(1)} %collective-permute-done.7), channel_id=1, source_target_pairs={{0,2},{1,3},{2,0},{3,1},{4,6},{5,7},{6,4},{7,5},{8,10},{9,11},{10,... | collective-permute-start | bytes 393224 | tf_op jit(solution)/shard_map/ppermute | solution.py:30
  26.8 21.6 %collective-permute-start.10 = (bf16[384,512]{1,0:T(8,128)(2,1)S(1)}, bf16[384,512]{1,0:T(8,128)(2,1)S(1)}, u32[]{:S(2)}, u32[]{:S(2)}) collective-permute-start(bf16[384,512]{1,0:T(8,128)(2,1)S(1)} %constant_dynamic-update-slice_fusion.refs_6_), channel_id=1, source_target_pairs={{0,8},{8,0},{16,24},{24,16},{1,9},{9,1},{17,25},{25,17},{2,10},{10... | collective-permute-start | bytes 1179656 | tf_op jit(solution)/shard_map/ppermute | solution.py:30
  29.2 19.8 %collective-permute-start.12 = (bf16[384,512]{1,0:T(8,128)(2,1)S(1)}, bf16[384,512]{1,0:T(8,128)(2,1)S(1)}, u32[]{:S(2)}, u32[]{:S(2)}) collective-permute-start(bf16[384,512]{1,0:T(8,128)(2,1)S(1)} %constant_dynamic-update-slice_fusion.refs_6_), channel_id=1, source_target_pairs={{0,16},{8,24},{16,0},{24,8},{1,17},{9,25},{17,1},{25,9},{2,18},{10... | collective-permute-start | bytes 1179656 | tf_op jit(solution)/shard_map/ppermute | solution.py:30
  30.7 18.3 %collective-permute-start.14 = (bf16[384,512]{1,0:T(8,128)(2,1)S(1)}, bf16[384,512]{1,0:T(8,128)(2,1)S(1)}, u32[]{:S(2)}, u32[]{:S(2)}) collective-permute-start(bf16[384,512]{1,0:T(8,128)(2,1)S(1)} %constant_dynamic-update-slice_fusion.refs_6_), channel_id=1, source_target_pairs={{0,24},{8,16},{16,8},{24,0},{1,25},{9,17},{17,9},{25,1},{2,26},{10... | collective-permute-start | bytes 1179656 | tf_op jit(solution)/shard_map/ppermute | solution.py:30
  31.6 4.3 %collective-permute-start.2 = (bf16[128,256]{1,0:T(8,128)(2,1)S(1)}, bf16[128,256]{1,0:T(8,128)(2,1)S(1)}, u32[]{:S(2)}, u32[]{:S(2)}) collective-permute-start(bf16[128,256]{1,0:T(8,128)(2,1)S(1)} %get-tuple-element.87), channel_id=1, source_target_pairs={{0,2},{1,3},{2,0},{3,1},{4,6},{5,7},{6,4},{7,5},{8,10},{9,11},{10,... | collective-permute-start | bytes 196616 | tf_op jit(solution)/shard_map/ppermute | solution.py:30
  32.1 17.3 %collective-permute-start.5 = (bf16[128,2048]{1,0:T(8,128)(2,1)S(1)}, bf16[128,2048]{1,0:T(8,128)(2,1)S(1)}, u32[]{:S(2)}, u32[]{:S(2)}) collective-permute-start(bf16[128,2048]{1,0:T(8,128)(2,1)S(1)} %copy-done.3), channel_id=1, source_target_pairs={{0,1},{1,0},{2,3},{3,2},{4,5},{5,4},{6,7},{7,6},{8,9},{9,8},{10,11... | collective-permute-start | bytes 1572872 | tf_op jit(solution)/shard_map/ppermute | solution.py:30
  35.9 6.4 %collective-permute-start.3 = (bf16[128,256]{1,0:T(8,128)(2,1)S(1)}, bf16[128,256]{1,0:T(8,128)(2,1)S(1)}, u32[]{:S(2)}, u32[]{:S(2)}) collective-permute-start(bf16[128,256]{1,0:T(8,128)(2,1)S(1)} %get-tuple-element.88), channel_id=1, source_target_pairs={{0,4},{1,5},{2,6},{3,7},{4,0},{5,1},{6,2},{7,3},{8,12},{9,13},{10,... | collective-permute-start | bytes 196616 | tf_op jit(solution)/shard_map/ppermute | solution.py:30
  42.4 6.1 %collective-permute-start.4 = (bf16[128,256]{1,0:T(8,128)(2,1)S(1)}, bf16[128,256]{1,0:T(8,128)(2,1)S(1)}, u32[]{:S(2)}, u32[]{:S(2)}) collective-permute-start(bf16[128,256]{1,0:T(8,128)(2,1)S(1)} %get-tuple-element.85), channel_id=1, source_target_pairs={{0,6},{1,7},{2,4},{3,5},{4,2},{5,3},{6,0},{7,1},{8,14},{9,15},{10,... | collective-permute-start | bytes 196616 | tf_op jit(solution)/shard_map/ppermute | solution.py:30
  48.4 1.7 collective-permute-start.9
  48.4 2.3 collective-permute-start.11
  48.9 2.3 collective-permute-start.13
  49.0 2.8 %collective-permute-start.15 = (bf16[384,512]{1,0:T(8,128)(2,1)S(1)}, bf16[384,512]{1,0:T(8,128)(2,1)S(1)}, u32[]{:S(2)}, u32[]{:S(2)}) collective-permute-start(bf16[384,512]{1,0:T(8,128)(2,1)S(1)} %collective-permute-done.14.refs_12_), channel_id=1, source_target_pairs={{0,1},{1,0},{2,3},{3,2},{4,5},{5,4},{6,7},{7,6},{8,9},{9,8},{10,11... | collective-permute-start | bytes 1179656 | tf_op jit(solution)/shard_map/ppermute | solution.py:30
  49.5 103.8 %collective-permute-start.30 = (bf16[768,2048]{1,0:T(8,128)(2,1)S(1)}, bf16[768,2048]{1,0:T(8,128)(2,1)}, u32[]{:S(2)}, u32[]{:S(2)}) collective-permute-start(bf16[768,2048]{1,0:T(8,128)(2,1)S(1)} %bitcast.80), channel_id=1, source_target_pairs={{0,1},{1,0},{2,3},{3,2},{4,5},{5,4},{6,7},{7,6},{8,9},{9,8},{10,11... | collective-permute-start | bytes 9437192 | tf_op jit(solution)/shard_map/ppermute | solution.py:30
  50.2 103.8 %collective-permute-start.31 = (bf16[768,2048]{1,0:T(8,128)(2,1)}, bf16[768,2048]{1,0:T(8,128)(2,1)}, u32[]{:S(2)}, u32[]{:S(2)}) collective-permute-start(bf16[768,2048]{1,0:T(8,128)(2,1)} %bitcast.85), channel_id=1, source_target_pairs={{0,1},{1,0},{2,3},{3,2},{4,5},{5,4},{6,7},{7,6},{8,9},{9,8},{10,11... | collective-permute-start | bytes 9437192 | tf_op jit(solution)/shard_map/ppermute | solution.py:30
  51.8 33.8 %copy-start.28 = (s32[1024,4]{0,1:T(4,128)S(1)}, s32[1024,4]{0,1:T(4,128)}, u32[]{:S(2)}) copy-start(s32[1024,4]{0,1:T(4,128)} %param.22) | copy-start | bytes 49156
  51.8 41.8 %copy-start.29 = (f32[1024,4]{0,1:T(4,128)S(1)}, f32[1024,4]{0,1:T(4,128)}, u32[]{:S(2)}) copy-start(f32[1024,4]{0,1:T(4,128)} %param.23) | copy-start | bytes 49156
  53.9 13.4 %collective-permute-start.24 = (bf16[128,1024]{1,0:T(8,128)(2,1)S(1)}, bf16[128,1024]{1,0:T(8,128)(2,1)}, u32[]{:S(2)}, u32[]{:S(2)}) collective-permute-start(bf16[128,1024]{1,0:T(8,128)(2,1)S(1)} %get-tuple-element.42.refs_1_), channel_id=1, source_target_pairs={{0,4},{1,5},{2,6},{3,7},{4,0},{5,1},{6,2},{7,3},{8,12},{9,13},{10,... | collective-permute-start | bytes 786440 | tf_op jit(solution)/shard_map/ppermute | solution.py:30
  53.9 14.1 %collective-permute-start.23 = (bf16[128,1024]{1,0:T(8,128)(2,1)S(1)}, bf16[128,1024]{1,0:T(8,128)(2,1)S(1)}, u32[]{:S(2)}, u32[]{:S(2)}) collective-permute-start(bf16[128,1024]{1,0:T(8,128)(2,1)S(1)} %get-tuple-element.42.refs_1_), channel_id=1, source_target_pairs={{0,2},{1,3},{2,0},{3,1},{4,6},{5,7},{6,4},{7,5},{8,10},{9,11},{10,... | collective-permute-start | bytes 786440 | tf_op jit(solution)/shard_map/ppermute | solution.py:30
  54.5 100.8 %collective-permute-start.32 = (bf16[768,2048]{1,0:T(8,128)(2,1)}, bf16[768,2048]{1,0:T(8,128)(2,1)}, u32[]{:S(2)}, u32[]{:S(2)}) collective-permute-start(bf16[768,2048]{1,0:T(8,128)(2,1)} %bitcast.41.refs_4_), channel_id=1, source_target_pairs={{0,1},{1,0},{2,3},{3,2},{4,5},{5,4},{6,7},{7,6},{8,9},{9,8},{10,11... | collective-permute-start | bytes 9437192 | tf_op jit(solution)/shard_map/ppermute | solution.py:30
  67.3 1.5 collective-permute-start.26
  68.0 14.5 %collective-permute-start.17 = (bf16[128,1024]{1,0:T(8,128)(2,1)S(1)}, bf16[128,1024]{1,0:T(8,128)(2,1)}, u32[]{:S(2)}, u32[]{:S(2)}) collective-permute-start(bf16[128,1024]{1,0:T(8,128)(2,1)S(1)} %get-tuple-element.40.refs_1_), channel_id=1, source_target_pairs={{0,4},{1,5},{2,6},{3,7},{4,0},{5,1},{6,2},{7,3},{8,12},{9,13},{10,... | collective-permute-start | bytes 786440 | tf_op jit(solution)/shard_map/ppermute | solution.py:30
  69.5 13.9 %collective-permute-start.16 = (bf16[128,1024]{1,0:T(8,128)(2,1)S(1)}, bf16[128,1024]{1,0:T(8,128)(2,1)S(1)}, u32[]{:S(2)}, u32[]{:S(2)}) collective-permute-start(bf16[128,1024]{1,0:T(8,128)(2,1)S(1)} %get-tuple-element.40.refs_1_), channel_id=1, source_target_pairs={{0,2},{1,3},{2,0},{3,1},{4,6},{5,7},{6,4},{7,5},{8,10},{9,11},{10,... | collective-permute-start | bytes 786440 | tf_op jit(solution)/shard_map/ppermute | solution.py:30
  82.5 1.5 collective-permute-start.19
  83.5 7.9 %collective-permute-start.25 = (bf16[128,1024]{1,0:T(8,128)(2,1)}, bf16[128,1024]{1,0:T(8,128)(2,1)S(1)}, u32[]{:S(2)}, u32[]{:S(2)}) collective-permute-start(bf16[128,1024]{1,0:T(8,128)(2,1)} %collective-permute-done.24.refs_3_), channel_id=1, source_target_pairs={{0,2},{1,3},{2,0},{3,1},{4,6},{5,7},{6,4},{7,5},{8,10},{9,11},{10,... | collective-permute-start | bytes 786440 | tf_op jit(solution)/shard_map/ppermute | solution.py:30
  84.9 6.5 %collective-permute-start.27 = (bf16[128,1024]{1,0:T(8,128)(2,1)S(1)}, bf16[128,1024]{1,0:T(8,128)(2,1)S(1)}, u32[]{:S(2)}, u32[]{:S(2)}) collective-permute-start(bf16[128,1024]{1,0:T(8,128)(2,1)S(1)} %collective-permute-done.23.refs_2_), channel_id=1, source_target_pairs={{0,1},{1,0},{2,3},{3,2},{4,5},{5,4},{6,7},{7,6},{8,9},{9,8},{10,11... | collective-permute-start | bytes 786440 | tf_op jit(solution)/shard_map/ppermute | solution.py:30
  91.4 5.3 %collective-permute-start.28 = (bf16[128,1024]{1,0:T(8,128)(2,1)}, bf16[128,1024]{1,0:T(8,128)(2,1)}, u32[]{:S(2)}, u32[]{:S(2)}) collective-permute-start(bf16[128,1024]{1,0:T(8,128)(2,1)} %collective-permute-done.24.refs_3_), channel_id=1, source_target_pairs={{0,1},{1,0},{2,3},{3,2},{4,5},{5,4},{6,7},{7,6},{8,9},{9,8},{10,11... | collective-permute-start | bytes 786440 | tf_op jit(solution)/shard_map/ppermute | solution.py:30
  92.8 8.4 %collective-permute-start.18 = (bf16[128,1024]{1,0:T(8,128)(2,1)}, bf16[128,1024]{1,0:T(8,128)(2,1)}, u32[]{:S(2)}, u32[]{:S(2)}) collective-permute-start(bf16[128,1024]{1,0:T(8,128)(2,1)} %collective-permute-done.17.refs_3_), channel_id=1, source_target_pairs={{0,2},{1,3},{2,0},{3,1},{4,6},{5,7},{6,4},{7,5},{8,10},{9,11},{10,... | collective-permute-start | bytes 786440 | tf_op jit(solution)/shard_map/ppermute | solution.py:30
  96.7 5.6 %collective-permute-start.20 = (bf16[128,1024]{1,0:T(8,128)(2,1)}, bf16[128,1024]{1,0:T(8,128)(2,1)S(1)}, u32[]{:S(2)}, u32[]{:S(2)}) collective-permute-start(bf16[128,1024]{1,0:T(8,128)(2,1)} %copy-done.9), channel_id=1, source_target_pairs={{0,1},{1,0},{2,3},{3,2},{4,5},{5,4},{6,7},{7,6},{8,9},{9,8},{10,11... | collective-permute-start | bytes 786440 | tf_op jit(solution)/shard_map/ppermute | solution.py:30
  101.2 2.4 collective-permute-start.29
  103.0 21.1 %collective-permute-start.21 = (bf16[128,1024]{1,0:T(8,128)(2,1)}, bf16[128,1024]{1,0:T(8,128)(2,1)}, u32[]{:S(2)}, u32[]{:S(2)}) collective-permute-start(bf16[128,1024]{1,0:T(8,128)(2,1)} %collective-permute-done.17.refs_3_), channel_id=1, source_target_pairs={{0,1},{1,0},{2,3},{3,2},{4,5},{5,4},{6,7},{7,6},{8,9},{9,8},{10,11... | collective-permute-start | bytes 786440 | tf_op jit(solution)/shard_map/ppermute | solution.py:30
  104.2 22.1 %collective-permute-start.22 = (bf16[128,1024]{1,0:T(8,128)(2,1)}, bf16[128,1024]{1,0:T(8,128)(2,1)}, u32[]{:S(2)}, u32[]{:S(2)}) collective-permute-start(bf16[128,1024]{1,0:T(8,128)(2,1)} %collective-permute-done.18.refs_4_), channel_id=1, source_target_pairs={{0,1},{1,0},{2,3},{3,2},{4,5},{5,4},{6,7},{7,6},{8,9},{9,8},{10,11... | collective-permute-start | bytes 786440 | tf_op jit(solution)/shard_map/ppermute | solution.py:30
  118.8 7.6 %copy-start.22 = (bf16[128,1024]{1,0:T(8,128)(2,1)S(1)}, bf16[128,1024]{1,0:T(8,128)(2,1)}, u32[]{:S(2)}) copy-start(bf16[128,1024]{1,0:T(8,128)(2,1)} %copy-done.21) | copy-start | bytes 786436
  124.1 15.8 %collective-permute-start.40 = (bf16[256,1024]{1,0:T(8,128)(2,1)S(1)}, bf16[256,1024]{1,0:T(8,128)(2,1)S(1)}, u32[]{:S(2)}, u32[]{:S(2)}) collective-permute-start(bf16[256,1024]{1,0:T(8,128)(2,1)S(1)} %get-tuple-element.52), channel_id=1, source_target_pairs={{0,24},{1,25},{2,26},{3,27},{4,28},{5,29},{6,30},{7,31},{8,16},{9,... | collective-permute-start | bytes 1572872 | tf_op jit(solution)/shard_map/ppermute | solution.py:427
  126.4 26.8 %copy-start.27 = (bf16[64,2048]{1,0:T(8,128)(2,1)S(1)}, bf16[64,2048]{1,0:T(8,128)(2,1)}, u32[]{:S(2)}) copy-start(bf16[64,2048]{1,0:T(8,128)(2,1)} %param.29) | copy-start | bytes 786436
  126.4 29.0 %copy-start.1 = (bf16[1,768,2048]{2,1,0:T(8,128)(2,1)S(1)}, bf16[1,768,2048]{2,1,0:T(8,128)(2,1)}, u32[]{:S(2)}) copy-start(bf16[1,768,2048]{2,1,0:T(8,128)(2,1)} %param.25) | copy-start | bytes 9437188
  131.9 19.2 %collective-permute-start.39 = (bf16[256,1024]{1,0:T(8,128)(2,1)S(1)}, bf16[256,1024]{1,0:T(8,128)(2,1)S(1)}, u32[]{:S(2)}, u32[]{:S(2)}) collective-permute-start(bf16[256,1024]{1,0:T(8,128)(2,1)S(1)} %get-tuple-element.51), channel_id=1, source_target_pairs={{0,24},{1,25},{2,26},{3,27},{4,28},{5,29},{6,30},{7,31},{8,16},{9,... | collective-permute-start | bytes 1572872 | tf_op jit(solution)/shard_map/ppermute | solution.py:427
  139.9 23.3 %collective-permute-start.37 = (bf16[256,1024]{1,0:T(8,128)(2,1)S(1)}, bf16[256,1024]{1,0:T(8,128)(2,1)S(1)}, u32[]{:S(2)}, u32[]{:S(2)}) collective-permute-start(bf16[256,1024]{1,0:T(8,128)(2,1)S(1)} %get-tuple-element.49), channel_id=1, source_target_pairs={{0,16},{1,9},{2,18},{3,11},{4,20},{5,13},{6,22},{7,15},{8,24},{9,1... | collective-permute-start | bytes 1572872 | tf_op jit(solution)/shard_map/ppermute | solution.py:427
  151.2 21.1 %collective-permute-start.36 = (bf16[256,1024]{1,0:T(8,128)(2,1)S(1)}, bf16[256,1024]{1,0:T(8,128)(2,1)S(1)}, u32[]{:S(2)}, u32[]{:S(2)}) collective-permute-start(bf16[256,1024]{1,0:T(8,128)(2,1)S(1)} %get-tuple-element.48), channel_id=1, source_target_pairs={{0,16},{1,9},{2,18},{3,11},{4,20},{5,13},{6,22},{7,15},{8,24},{9,1... | collective-permute-start | bytes 1572872 | tf_op jit(solution)/shard_map/ppermute | solution.py:427
  153.2 29.5 %collective-permute-start.34 = (bf16[256,1024]{1,0:T(8,128)(2,1)S(1)}, bf16[256,1024]{1,0:T(8,128)(2,1)S(1)}, u32[]{:S(2)}, u32[]{:S(2)}) collective-permute-start(bf16[256,1024]{1,0:T(8,128)(2,1)S(1)} %get-tuple-element.46), channel_id=1, source_target_pairs={{0,8},{1,17},{2,10},{3,19},{4,12},{5,21},{6,14},{7,23},{8,0},{9,25... | collective-permute-start | bytes 1572872 | tf_op jit(solution)/shard_map/ppermute | solution.py:427
  154.0 28.7 %collective-permute-start.33 = (bf16[256,1024]{1,0:T(8,128)(2,1)S(1)}, bf16[256,1024]{1,0:T(8,128)(2,1)S(1)}, u32[]{:S(2)}, u32[]{:S(2)}) collective-permute-start(bf16[256,1024]{1,0:T(8,128)(2,1)S(1)} %get-tuple-element.45), channel_id=1, source_target_pairs={{0,8},{1,17},{2,10},{3,19},{4,12},{5,21},{6,14},{7,23},{8,0},{9,25... | collective-permute-start | bytes 1572872 | tf_op jit(solution)/shard_map/ppermute | solution.py:427
  162.6 31.1 %collective-permute-start.48 = (bf16[256,1024]{1,0:T(8,128)(2,1)S(1)}, bf16[256,1024]{1,0:T(8,128)(2,1)S(1)}, u32[]{:S(2)}, u32[]{:S(2)}) collective-permute-start(bf16[256,1024]{1,0:T(8,128)(2,1)S(1)} %get-tuple-element.66), channel_id=1, source_target_pairs={{0,24},{1,25},{2,26},{3,27},{4,28},{5,29},{6,30},{7,31},{8,16},{9,... | collective-permute-start | bytes 1572872 | tf_op jit(solution)/shard_map/ppermute | solution.py:427
  179.8 21.9 %collective-permute-start.47 = (bf16[256,1024]{1,0:T(8,128)(2,1)S(1)}, bf16[256,1024]{1,0:T(8,128)(2,1)S(1)}, u32[]{:S(2)}, u32[]{:S(2)}) collective-permute-start(bf16[256,1024]{1,0:T(8,128)(2,1)S(1)} %get-tuple-element.65), channel_id=1, source_target_pairs={{0,16},{1,9},{2,18},{3,11},{4,20},{5,13},{6,22},{7,15},{8,24},{9,1... | collective-permute-start | bytes 1572872 | tf_op jit(solution)/shard_map/ppermute | solution.py:427
  190.0 14.9 %collective-permute-start.46 = (bf16[256,1024]{1,0:T(8,128)(2,1)S(1)}, bf16[256,1024]{1,0:T(8,128)(2,1)S(1)}, u32[]{:S(2)}, u32[]{:S(2)}) collective-permute-start(bf16[256,1024]{1,0:T(8,128)(2,1)S(1)} %get-tuple-element.64), channel_id=1, source_target_pairs={{0,8},{1,17},{2,10},{3,19},{4,12},{5,21},{6,14},{7,23},{8,0},{9,25... | collective-permute-start | bytes 1572872 | tf_op jit(solution)/shard_map/ppermute | solution.py:427
  190.2 23.7 %collective-permute-start.41 = (bf16[256,1024]{1,0:T(8,128)(2,1)S(1)}, bf16[256,1024]{1,0:T(8,128)(2,1)S(1)}, u32[]{:S(2)}, u32[]{:S(2)}) collective-permute-start(bf16[256,1024]{1,0:T(8,128)(2,1)S(1)} %get-tuple-element.53), channel_id=1, source_target_pairs={{0,24},{1,25},{2,26},{3,27},{4,28},{5,29},{6,30},{7,31},{8,16},{9,... | collective-permute-start | bytes 1572872 | tf_op jit(solution)/shard_map/ppermute | solution.py:427
  191.8 26.8 %collective-permute-start.38 = (bf16[256,1024]{1,0:T(8,128)(2,1)S(1)}, bf16[256,1024]{1,0:T(8,128)(2,1)S(1)}, u32[]{:S(2)}, u32[]{:S(2)}) collective-permute-start(bf16[256,1024]{1,0:T(8,128)(2,1)S(1)} %get-tuple-element.50), channel_id=1, source_target_pairs={{0,16},{1,9},{2,18},{3,11},{4,20},{5,13},{6,22},{7,15},{8,24},{9,1... | collective-permute-start | bytes 1572872 | tf_op jit(solution)/shard_map/ppermute | solution.py:427
  193.8 25.0 %collective-permute-start.35 = (bf16[256,1024]{1,0:T(8,128)(2,1)S(1)}, bf16[256,1024]{1,0:T(8,128)(2,1)S(1)}, u32[]{:S(2)}, u32[]{:S(2)}) collective-permute-start(bf16[256,1024]{1,0:T(8,128)(2,1)S(1)} %get-tuple-element.47), channel_id=1, source_target_pairs={{0,8},{1,17},{2,10},{3,19},{4,12},{5,21},{6,14},{7,23},{8,0},{9,25... | collective-permute-start | bytes 1572872 | tf_op jit(solution)/shard_map/ppermute | solution.py:427
  206.6 15.9 %collective-permute-start.49 = (bf16[512,1024]{1,0:T(8,128)(2,1)S(1)}, bf16[512,1024]{1,0:T(8,128)(2,1)S(1)}, u32[]{:S(2)}, u32[]{:S(2)}) collective-permute-start(bf16[512,1024]{1,0:T(8,128)(2,1)S(1)} %combine.6), channel_id=1, source_target_pairs={{0,1},{1,0},{2,3},{3,2},{4,5},{5,4},{6,7},{7,6},{8,9},{9,8},{10,11... | collective-permute-start | bytes 3145736 | tf_op jit(solution)/shard_map/ppermute | solution.py:30
  220.6 4.2 %collective-permute-start.42 = (bf16[512,1024]{1,0:T(8,128)(2,1)S(1)}, bf16[512,1024]{1,0:T(8,128)(2,1)S(1)}, u32[]{:S(2)}, u32[]{:S(2)}) collective-permute-start(bf16[512,1024]{1,0:T(8,128)(2,1)S(1)} %combine.4), channel_id=1, source_target_pairs={{0,1},{1,0},{2,3},{3,2},{4,5},{5,4},{6,7},{7,6},{8,9},{9,8},{10,11... | collective-permute-start | bytes 3145736 | tf_op jit(solution)/shard_map/ppermute | solution.py:30
  224.3 39.2 %copy-start.6 = (bf16[128,2048]{1,0:T(8,128)(2,1)S(1)}, bf16[128,2048]{1,0:T(8,128)(2,1)}, u32[]{:S(2)}) copy-start(bf16[128,2048]{1,0:T(8,128)(2,1)} %copy-done.5) | copy-start | bytes 1572868
  224.3 9.2 %collective-permute-start.51 = (bf16[128,1024]{1,0:T(8,128)(2,1)S(1)}, bf16[128,1024]{1,0:T(8,128)(2,1)S(1)}, u32[]{:S(2)}, u32[]{:S(2)}) collective-permute-start(bf16[128,1024]{1,0:T(8,128)(2,1)S(1)} %get-tuple-element.70), channel_id=1, source_target_pairs={{0,2},{1,3},{2,0},{3,1},{4,6},{5,7},{6,4},{7,5},{8,10},{9,11},{10,... | collective-permute-start | bytes 786440 | tf_op jit(solution)/shard_map/ppermute | solution.py:30
  226.6 18.2 %collective-permute-start.44 = (bf16[128,1024]{1,0:T(8,128)(2,1)S(1)}, bf16[128,1024]{1,0:T(8,128)(2,1)S(1)}, u32[]{:S(2)}, u32[]{:S(2)}) collective-permute-start(bf16[128,1024]{1,0:T(8,128)(2,1)S(1)} %get-tuple-element.62), channel_id=1, source_target_pairs={{0,2},{1,3},{2,0},{3,1},{4,6},{5,7},{6,4},{7,5},{8,10},{9,11},{10,... | collective-permute-start | bytes 786440 | tf_op jit(solution)/shard_map/ppermute | solution.py:30
  228.2 25.1 %collective-permute-start.50 = (bf16[128,1024]{1,0:T(8,128)(2,1)S(1)}, bf16[128,1024]{1,0:T(8,128)(2,1)S(1)}, u32[]{:S(2)}, u32[]{:S(2)}) collective-permute-start(bf16[128,1024]{1,0:T(8,128)(2,1)S(1)} %get-tuple-element.68), channel_id=1, source_target_pairs={{0,2},{1,3},{2,0},{3,1},{4,6},{5,7},{6,4},{7,5},{8,10},{9,11},{10,... | collective-permute-start | bytes 786440 | tf_op jit(solution)/shard_map/ppermute | solution.py:30
  228.7 29.4 %collective-permute-start.43 = (bf16[128,1024]{1,0:T(8,128)(2,1)S(1)}, bf16[128,1024]{1,0:T(8,128)(2,1)S(1)}, u32[]{:S(2)}, u32[]{:S(2)}) collective-permute-start(bf16[128,1024]{1,0:T(8,128)(2,1)S(1)} %get-tuple-element.60), channel_id=1, source_target_pairs={{0,2},{1,3},{2,0},{3,1},{4,6},{5,7},{6,4},{7,5},{8,10},{9,11},{10,... | collective-permute-start | bytes 786440 | tf_op jit(solution)/shard_map/ppermute | solution.py:30
  233.6 24.4 %collective-permute-start.52 = (bf16[128,1024]{1,0:T(8,128)(2,1)S(1)}, bf16[128,1024]{1,0:T(8,128)(2,1)S(1)}, u32[]{:S(2)}, u32[]{:S(2)}) collective-permute-start(bf16[128,1024]{1,0:T(8,128)(2,1)S(1)} %add_convert_fusion.1), channel_id=1, source_target_pairs={{0,4},{1,5},{2,6},{3,7},{4,0},{5,1},{6,2},{7,3},{8,12},{9,13},{10,... | collective-permute-start | bytes 786440 | tf_op jit(solution)/shard_map/ppermute | solution.py:30
  244.8 18.7 %collective-permute-start.45 = (bf16[128,1024]{1,0:T(8,128)(2,1)S(1)}, bf16[128,1024]{1,0:T(8,128)(2,1)S(1)}, u32[]{:S(2)}, u32[]{:S(2)}) collective-permute-start(bf16[128,1024]{1,0:T(8,128)(2,1)S(1)} %add_convert_fusion.3), channel_id=1, source_target_pairs={{0,4},{1,5},{2,6},{3,7},{4,0},{5,1},{6,2},{7,3},{8,12},{9,13},{10,... | collective-permute-start | bytes 786440 | tf_op jit(solution)/shard_map/ppermute | solution.py:30
  (20 other events, 30.5 us)
where the time goes:
time: 265 us
  waiting for transfers between devices  130 us (49%)
  Pallas kernels  53.4 us (20%)
  starting transfers between devices  46 us (17%)
  local copies, waits for them, and re-layouts  27.6 us (10%)
  other arithmetic  6.01 us (2%)
    ppermute x40, waiting for transfers between devices, peer(): return lax.ppermute(x, axis, [(i, i ^ step) for i in range(count)])  91.5 us
    ppermute x12, waiting for transfers between devices, cross(): return lax.ppermute(x, ('sp', 'tp'), route)  37.6 us
    pallas_call x4, Pallas kernels, expert(): pl.pallas_call(kernel, out_shape=[jax.ShapeDtypeStruct((rows, part), jnp....  29.6 us
    ppermute x40, starting transfers between devices, peer(): return lax.ppermute(x, axis, [(i, i ^ step) for i in range(count)])  26.3 us
    ppermute x12, starting transfers between devices, cross(): return lax.ppermute(x, ('sp', 'tp'), route)  16.3 us
    unnamed x66, local copies, waits for them, and re-layouts  14.6 us
    pallas_call x2, Pallas kernels, pick_rows(): pl.pallas_call(kernel, out_shape=[jax.ShapeDtypeStruct((half_cap, part),...  10.9 us
    pallas_call x4, Pallas kernels, combine(): pl.pallas_call(kernel, grid=(1,), out_shape=[jax.ShapeDtypeStruct((rows /...  7.13 us
  transfers between devices with their start and end apart: 53, of which 30 were waited for; matrix products, arithmetic and copies ran while one was open for 7% of the time, Pallas kernels for 20%

commit v1 on v0

--- a/solution.py
+++ b/solution.py
@@ -342,13 +342,13 @@
             rows_v[i * rows : (i + 1) * rows] = parts[i][...]
 
         def columns(t, carry):
-            at = pl.ds(pl.multiple_of(t * 256, 256), 256)
+            at = pl.ds(pl.multiple_of(t * 512, 512), 512)
             for step in range(sp_count):
                 slots = pl.ds(step * half_cap, half_cap)
                 outs[step][:, at] = dot(pick_r[slots], rows_v[:, at]).astype(jnp.bfloat16)
             return carry
 
-        lax.fori_loop(0, part // 256, columns, 0)
+        lax.fori_loop(0, part // 512, columns, 0)
         gate_o[...] = dot_t(rows_v[...], gate_r[...])
         up_o[...] = dot_t(rows_v[...], up_r[...])
 
@@ -364,12 +364,13 @@
     )(pick, *blocks, gate, up)
 
 
-def combine(mix, held, hidden, down, half, arrived):
+def combine(mix, held, hidden, down, half):
     rows = mix.shape[0] // 2
     sp_count = len(held)
     half_cap, part = held[0].shape
     chips = lax.axis_size("tp") // 2
-    outs_n = 1 if arrived is None else chips
+    outs_n = 1 if half else chips
+    kind = jnp.bfloat16 if half else jnp.float32
 
     def kernel(*refs):
         mix_r, parts, hid, down_r = refs[0], refs[1 : 1 + sp_count], *refs[1 + sp_count : 3 + sp_count]
@@ -382,9 +383,7 @@
         def columns(t, carry):
             at = pl.ds(pl.multiple_of(t * 512, 512), 512)
             total = dot(mix_r[...], held_v[:, at]) + dot(hid[...], down_r[:, at])
-            if arrived is not None:
-                total = total + refs[3 + sp_count][:, at].astype(jnp.float32)
-            total = total.astype(jnp.bfloat16)
+            total = total.astype(kind)
             for i in range(outs_n):
                 outs[i][:, at] = total[i * each : (i + 1) * each]
             return carry
@@ -395,20 +394,18 @@
         return pl.BlockSpec((rows, x.shape[1]), lambda i: (half, 0))
 
     full = lambda x: pl.BlockSpec(x.shape, lambda i: (0, 0))
-    more = [] if arrived is None else [arrived]
     return pl.pallas_call(
         kernel,
         grid=(1,),
-        out_shape=[jax.ShapeDtypeStruct((rows // outs_n, part), jnp.bfloat16)] * outs_n,
+        out_shape=[jax.ShapeDtypeStruct((rows // outs_n, part), kind)] * outs_n,
         in_specs=[block(mix)]
         + [full(x) for x in held]
-        + [block(hidden), full(down)]
-        + [full(x) for x in more],
+        + [block(hidden), full(down)],
         out_specs=[pl.BlockSpec((rows // outs_n, part), lambda i: (0, 0))] * outs_n,
         scratch_shapes=[pltpu.VMEM((sp_count * half_cap, part), jnp.bfloat16)],
         compiler_params=ROOMY,
         name="combine",
-    )(mix, *held, hidden, down, *more)
+    )(mix, *held, hidden, down)
 
 
 def crossing(step, core):
@@ -505,10 +502,13 @@
     for c in range(CHUNKS):
         back = [held[step][c] for step in range(sp_count)]
         down = shared_down[:, cuts[c]]
-        (for_mate,) = combine(mix, back, shared_hidden, down, 1, None)
+        (for_mate,) = combine(mix, back, shared_hidden, down, 1)
         from_mate = peer(for_mate, "tp", 1)
-        sums = combine(mix, back, shared_hidden, down, 0, from_mate)
-        sums = [x.astype(jnp.float32) for x in sums]
+        sums = combine(mix, back, shared_hidden, down, 0)
+        sums = [
+            x + from_mate[k * own_rows : (k + 1) * own_rows].astype(jnp.float32)
+            for k, x in enumerate(sums)
+        ]
         sums[0] = sums[0] + after_mix[:, cuts[c]].astype(jnp.float32)
         for bit in reversed(high_bits(chips)):
             for k in range(0, chips, 2 * bit):

time: 265 us -> 267 us (level)
  transfers between devices with their start and end apart: 53 -> 53, of which waited for: 30 -> 29; matrix products, arithmetic and copies ran while one was open for 7% -> 7% of each run, Pallas kernels for 20% -> 20%
where the time goes in v1:
time: 267 us; the launch traced here: 266 us
  waiting for transfers between devices  131 us (49%)
  Pallas kernels  52.7 us (20%)
  starting transfers between devices  46.2 us (17%)
  local copies, waits for them, and re-layouts  27.7 us (10%)
  other arithmetic  6.47 us (2%)
    ppermute x40, waiting for transfers between devices, peer(): return lax.ppermute(x, axis, [(i, i ^ step) for i in range(count)])  92.9 us
    ppermute x12, waiting for transfers between devices, cross(): return lax.ppermute(x, ('sp', 'tp'), route)  37.9 us
    pallas_call x4, Pallas kernels, expert(): pl.pallas_call(kernel, out_shape=[jax.ShapeDtypeStruct((rows, part), jnp....  29.6 us
    ppermute x40, starting transfers between devices, peer(): return lax.ppermute(x, axis, [(i, i ^ step) for i in range(count)])  26.4 us
    ppermute x12, starting transfers between devices, cross(): return lax.ppermute(x, ('sp', 'tp'), route)  16.4 us
    unnamed x66, local copies, waits for them, and re-layouts  14.6 us
    pallas_call x2, Pallas kernels, pick_rows(): pl.pallas_call(kernel, out_shape=[jax.ShapeDtypeStruct((half_cap, part),...  10.2 us
    pallas_call x4, Pallas kernels, combine(): pl.pallas_call(kernel, grid=(1,), out_shape=[jax.ShapeDtypeStruct((rows /...  7.12 us
  transfers between devices with their start and end apart: 53, of which 29 were waited for; matrix products, arithmetic and copies ran while one was open for 7% of the time, Pallas kernels for 20%

profile of v1, /device:TPU:0, one launch (start us, length us, event | category | flops | bytes accessed | tf_op | source)
XLA Modules:
  0.0 266.4 jit_solution(556470384783868005)
XLA Ops:
  0.0 1.6 constant_dynamic-slice_fusion
  1.6 4.1 %collective-permute-start.7 = (bf16[128,512]{1,0:T(8,128)(2,1)}, bf16[128,512]{1,0:T(8,128)(2,1)S(1)}, u32[]{:S(2)}, u32[]{:S(2)}) collective-permute-start(bf16[128,512]{1,0:T(8,128)(2,1)} %constant_dynamic-slice_fusion), channel_id=1, source_target_pairs={{0,4},{1,5},{2,6},{3,7},{4,0},{5,1},{6,2},{7,3},{8,12},{9,13},{10,... | collective-permute-start | bytes 393224 | tf_op jit(solution)/shard_map/ppermute | solution.py:30
  5.7 1.6 collective-permute-start.6
  7.2 1.2 constant_dynamic-slice_fusion.1
  8.8 3.4 %collective-permute-start = (bf16[128,128]{0,1:T(8,128)(2,1)S(1)}, bf16[128,128]{0,1:T(8,128)(2,1)S(1)}, u32[]{:S(2)}, u32[]{:S(2)}) collective-permute-start(bf16[128,128]{0,1:T(8,128)(2,1)S(1)} %pad_maximum_fusion.2), channel_id=1, source_target_pairs={{0,8},{8,16},{16,24},{1,9},{9,17},{17,25},{2,10},{10,18},{18,26},{... | collective-permute-start | bytes 98312 | tf_op jit(solution)/shard_map/ppermute | solution.py:23
  16.8 1.9 copy.42
  19.6 1.1 select_select_fusion.1
  22.4 4.4 %collective-permute-done.8 = bf16[128,512]{1,0:T(8,128)(2,1)S(1)} collective-permute-done((bf16[128,512]{1,0:T(8,128)(2,1)S(1)}, bf16[128,512]{1,0:T(8,128)(2,1)S(1)}, u32[]{:S(2)}, u32[]{:S(2)}) %collective-permute-start.8) | collective-permute-done | bytes 131104 | tf_op jit(solution)/shard_map/ppermute | solution.py:30
  26.8 2.4 collective-permute-start.10
  29.2 1.5 collective-permute-start.12
  32.1 3.8 %collective-permute-done.2.refs_1_ = bf16[128,256]{1,0:T(8,128)(2,1)S(1)} collective-permute-done((bf16[128,256]{1,0:T(8,128)(2,1)S(1)}, bf16[128,256]{1,0:T(8,128)(2,1)S(1)}, u32[]{:S(2)}, u32[]{:S(2)}) %collective-permute-start.2) | collective-permute-done | bytes 65568 | tf_op jit(solution)/shard_map/ppermute | solution.py:30
  36.4 6.0 %collective-permute-done.3.refs_2_ = bf16[128,256]{1,0:T(8,128)(2,1)S(1)} collective-permute-done((bf16[128,256]{1,0:T(8,128)(2,1)S(1)}, bf16[128,256]{1,0:T(8,128)(2,1)S(1)}, u32[]{:S(2)}, u32[]{:S(2)}) %collective-permute-start.3) | collective-permute-done | bytes 65568 | tf_op jit(solution)/shard_map/ppermute | solution.py:30
  42.4 6.1 %collective-permute-done.4.refs_3_ = bf16[128,256]{1,0:T(8,128)(2,1)S(1)} collective-permute-done((bf16[128,256]{1,0:T(8,128)(2,1)S(1)}, bf16[128,256]{1,0:T(8,128)(2,1)S(1)}, u32[]{:S(2)}, u32[]{:S(2)}) %collective-permute-start.4) | collective-permute-done | bytes 65568 | tf_op jit(solution)/shard_map/ppermute | solution.py:30
  51.9 1.2 project.1
  54.5 12.8 %collective-permute-done.24.refs_3_ = bf16[128,1024]{1,0:T(8,128)(2,1)} collective-permute-done((bf16[128,1024]{1,0:T(8,128)(2,1)S(1)}, bf16[128,1024]{1,0:T(8,128)(2,1)}, u32[]{:S(2)}, u32[]{:S(2)}) %collective-permute-start.24) | collective-permute-done | bytes 262176 | tf_op jit(solution)/shard_map/ppermute | solution.py:30
  69.6 1.4 collective-permute-start.16
  71.0 11.5 %collective-permute-done.17.refs_3_ = bf16[128,1024]{1,0:T(8,128)(2,1)} collective-permute-done((bf16[128,1024]{1,0:T(8,128)(2,1)S(1)}, bf16[128,1024]{1,0:T(8,128)(2,1)}, u32[]{:S(2)}, u32[]{:S(2)}) %collective-permute-start.17) | collective-permute-done | bytes 262176 | tf_op jit(solution)/shard_map/ppermute | solution.py:30
  82.6 1.0 collective-permute-done.16.refs_2_
  86.1 5.3 %collective-permute-done.25.refs_4_ = bf16[128,1024]{1,0:T(8,128)(2,1)S(1)} collective-permute-done((bf16[128,1024]{1,0:T(8,128)(2,1)}, bf16[128,1024]{1,0:T(8,128)(2,1)S(1)}, u32[]{:S(2)}, u32[]{:S(2)}) %collective-permute-start.25) | collective-permute-done | bytes 262176 | tf_op jit(solution)/shard_map/ppermute | solution.py:30
  93.8 1.0 copy.28
  94.8 1.0 copy.29
  95.8 1.0 copy.30
  96.8 4.5 %collective-permute-done.18.refs_4_ = bf16[128,1024]{1,0:T(8,128)(2,1)} collective-permute-done((bf16[128,1024]{1,0:T(8,128)(2,1)}, bf16[128,1024]{1,0:T(8,128)(2,1)}, u32[]{:S(2)}, u32[]{:S(2)}) %collective-permute-start.18) | collective-permute-done | bytes 262176 | tf_op jit(solution)/shard_map/ppermute | solution.py:30
  101.2 1.1 select_select_fusion
  105.1 1.2 copy.31.table_r
  106.3 1.1 copy-done.2
  107.4 4.6 %matrices.1 = (bf16[1024,1024]{1,0:T(8,128)(2,1)S(1)}, bf16[1024,1024]{1,0:T(8,128)(2,1)S(1)}) custom-call(f32[8,1024]{1,0:T(8,128)S(1)} %copy.31.table_r, f32[1024,8]{1,0:T(8,128)S(1)} %bitcast.91), custom_call_target="tpu_custom_call" | custom-call | tf_op jit(solution)/shard_map/matrices/pallas_call | solution.py:147
  112.0 1.1 fusion.58
  114.1 0.9 copy-done.12
  115.0 0.9 copy-done.16
  116.9 0.9 copy-done.20
  117.9 0.9 copy-done.24
  118.8 5.0 %pick_rows.3 = (bf16[256,1024]{1,0:T(8,128)(2,1)S(1)}, bf16[256,1024]{1,0:T(8,128)(2,1)S(1)}, bf16[256,1024]{1,0:T(8,128)(2,1)S(1)}, bf16[256,1024]{1,0:T(8,128)...) custom-call(bf16[1024,1024]{1,0:T(8,128)(2,1)S(1)} %get-tuple-element.39.refs_0_, ...), custom_call_target="tpu_custom_call" | custom-call | tf_op jit(solution)/shard_map/pick_rows/pallas_call | solution.py:355
  123.8 2.2 collective-permute-start.40
  126.1 5.2 %pick_rows.2 = (bf16[256,1024]{1,0:T(8,128)(2,1)S(1)}, bf16[256,1024]{1,0:T(8,128)(2,1)S(1)}, bf16[256,1024]{1,0:T(8,128)(2,1)S(1)}, bf16[256,1024]{1,0:T(8,128)...) custom-call(bf16[1024,1024]{1,0:T(8,128)(2,1)S(1)} %get-tuple-element.39.refs_0_, ...), custom_call_target="tpu_custom_call" | custom-call | tf_op jit(solution)/shard_map/pick_rows/pallas_call | solution.py:355
  132.1 7.4 %collective-permute-done.40.refs_1_ = bf16[256,1024]{1,0:T(8,128)(2,1)S(1)} collective-permute-done((bf16[256,1024]{1,0:T(8,128)(2,1)S(1)}, bf16[256,1024]{1,0:T(8,128)(2,1)S(1)}, u32[]{:S(2)}, u32[]{:S(2)}) %collective-permute-start.40) | collective-permute-done | bytes 524320 | tf_op jit(solution)/shard_map/ppermute | solution.py:424
  139.6 2.0 collective-permute-start.37
  141.6 9.2 %collective-permute-done.39.refs_0_ = bf16[256,1024]{1,0:T(8,128)(2,1)S(1)} collective-permute-done((bf16[256,1024]{1,0:T(8,128)(2,1)S(1)}, bf16[256,1024]{1,0:T(8,128)(2,1)S(1)}, u32[]{:S(2)}, u32[]{:S(2)}) %collective-permute-start.39) | collective-permute-done | bytes 524320 | tf_op jit(solution)/shard_map/ppermute | solution.py:424
  150.8 2.0 collective-permute-start.36
  153.7 1.4 collective-permute-start.33
  155.0 7.3 %expert.7 = (bf16[256,1024]{1,0:T(8,128)(2,1)S(1)}, bf16[256,1024]{1,0:T(8,128)(2,1)S(1)}) custom-call(bf16[256,1024]{1,0:T(8,128)(2,1)S(1)} %collective-permute-done.39.refs_0_, bf16[256,1024]{1,0:T(8,128)(2,1)S(1)} %collective-permute-done.40.refs_1_, bf16[768,2048]{1,0:T(8,128)(2,1)S(1)} %bitcast.81, bf16[768,2048]{1,0:T(8,128)(2,1)S(1)} %bitcast.86, ...), custom_call_target="tpu_custom_call" | custom-call | flops 4831838208 | bytes 20971520 | tf_op jit(solution)/shard_map/expert/pallas_call | solution.py:248
  162.9 9.0 %collective-permute-done.36.refs_0_ = bf16[256,1024]{1,0:T(8,128)(2,1)S(1)} collective-permute-done((bf16[256,1024]{1,0:T(8,128)(2,1)S(1)}, bf16[256,1024]{1,0:T(8,128)(2,1)S(1)}, u32[]{:S(2)}, u32[]{:S(2)}) %collective-permute-start.36) | collective-permute-done | bytes 524320 | tf_op jit(solution)/shard_map/ppermute | solution.py:424
  171.9 7.5 %expert.6 = (bf16[256,1024]{1,0:T(8,128)(2,1)S(1)}, bf16[256,1024]{1,0:T(8,128)(2,1)S(1)}) custom-call(bf16[256,1024]{1,0:T(8,128)(2,1)S(1)} %collective-permute-done.36.refs_0_, bf16[256,1024]{1,0:T(8,128)(2,1)S(1)} %collective-permute-done.37.refs_1_, bf16[768,2048]{1,0:T(8,128)(2,1)S(1)} %bitcast.82, bf16[768,2048]{1,0:T(8,128)(2,1)S(1)} %bitcast.87, ...), custom_call_target="tpu_custom_call" | custom-call | flops 4831838208 | bytes 20971520 | tf_op jit(solution)/shard_map/expert/pallas_call | solution.py:248
  179.4 2.9 %collective-permute-start.47 = (bf16[256,1024]{1,0:T(8,128)(2,1)S(1)}, bf16[256,1024]{1,0:T(8,128)(2,1)S(1)}, u32[]{:S(2)}, u32[]{:S(2)}) collective-permute-start(bf16[256,1024]{1,0:T(8,128)(2,1)S(1)} %get-tuple-element.65), channel_id=1, source_target_pairs={{0,16},{1,9},{2,18},{3,11},{4,20},{5,13},{6,22},{7,15},{8,24},{9,1... | collective-permute-start | bytes 1572872 | tf_op jit(solution)/shard_map/ppermute | solution.py:424
  182.4 7.3 %expert.5 = (bf16[256,1024]{1,0:T(8,128)(2,1)S(1)}, bf16[256,1024]{1,0:T(8,128)(2,1)S(1)}) custom-call(bf16[256,1024]{1,0:T(8,128)(2,1)S(1)} %collective-permute-done.33.refs_0_, bf16[256,1024]{1,0:T(8,128)(2,1)S(1)} %collective-permute-done.34.refs_1_, bf16[768,2048]{1,0:T(8,128)(2,1)S(1)} %bitcast.83, bf16[768,2048]{1,0:T(8,128)(2,1)S(1)} %bitcast.88, ...), custom_call_target="tpu_custom_call" | custom-call | flops 4831838208 | bytes 20971520 | tf_op jit(solution)/shard_map/expert/pallas_call | solution.py:248
  189.9 1.5 collective-permute-start.41
  191.5 2.0 collective-permute-start.38
  193.5 7.5 %expert.4 = (bf16[256,1024]{1,0:T(8,128)(2,1)S(1)}, bf16[256,1024]{1,0:T(8,128)(2,1)S(1)}) custom-call(bf16[256,1024]{1,0:T(8,128)(2,1)S(1)} %get-tuple-element.41.refs_0_, bf16[256,1024]{1,0:T(8,128)(2,1)S(1)} %get-tuple-element.43.refs_1_, bf16[768,2048]{1,0:T(8,128)(2,1)S(1)} %bitcast.84, bf16[768,2048]{1,0:T(8,128)(2,1)S(1)} %bitcast.89, ...), custom_call_target="tpu_custom_call" | custom-call | flops 4831838208 | bytes 20971520 | tf_op jit(solution)/shard_map/expert/pallas_call | solution.py:248
  201.4 3.1 %collective-permute-done.46.refs_2_ = bf16[256,1024]{1,0:T(8,128)(2,1)S(1)} collective-permute-done((bf16[256,1024]{1,0:T(8,128)(2,1)S(1)}, bf16[256,1024]{1,0:T(8,128)(2,1)S(1)}, u32[]{:S(2)}, u32[]{:S(2)}) %collective-permute-start.46) | collective-permute-done | bytes 524320 | tf_op jit(solution)/shard_map/ppermute | solution.py:424
  204.5 1.8 combine.7
  206.3 3.5 %collective-permute-start.49 = (bf16[512,1024]{1,0:T(8,128)(2,1)S(1)}, bf16[512,1024]{1,0:T(8,128)(2,1)S(1)}, u32[]{:S(2)}, u32[]{:S(2)}) collective-permute-start(bf16[512,1024]{1,0:T(8,128)(2,1)S(1)} %combine.7), channel_id=1, source_target_pairs={{0,1},{1,0},{2,3},{3,2},{4,5},{5,4},{6,7},{7,6},{8,9},{9,8},{10,11... | collective-permute-start | bytes 3145736 | tf_op jit(solution)/shard_map/ppermute | solution.py:30
  209.8 3.8 %collective-permute-done.41.refs_4_ = bf16[256,1024]{1,0:T(8,128)(2,1)S(1)} collective-permute-done((bf16[256,1024]{1,0:T(8,128)(2,1)S(1)}, bf16[256,1024]{1,0:T(8,128)(2,1)S(1)}, u32[]{:S(2)}, u32[]{:S(2)}) %collective-permute-start.41) | collective-permute-done | bytes 524320 | tf_op jit(solution)/shard_map/ppermute | solution.py:424
  213.6 4.6 %collective-permute-done.38.refs_3_ = bf16[256,1024]{1,0:T(8,128)(2,1)S(1)} collective-permute-done((bf16[256,1024]{1,0:T(8,128)(2,1)S(1)}, bf16[256,1024]{1,0:T(8,128)(2,1)S(1)}, u32[]{:S(2)}, u32[]{:S(2)}) %collective-permute-start.38) | collective-permute-done | bytes 524320 | tf_op jit(solution)/shard_map/ppermute | solution.py:424
  218.5 1.8 combine.5
  220.3 1.9 collective-permute-start.42
  222.2 1.8 combine.6
  224.0 1.8 combine.4
  226.4 1.8 collective-permute-start.44
  228.5 1.7 collective-permute-start.43
  230.3 4.9 %collective-permute-done.51 = bf16[128,1024]{1,0:T(8,128)(2,1)S(1)} collective-permute-done((bf16[128,1024]{1,0:T(8,128)(2,1)S(1)}, bf16[128,1024]{1,0:T(8,128)(2,1)S(1)}, u32[]{:S(2)}, u32[]{:S(2)}) %collective-permute-start.51) | collective-permute-done | bytes 262176 | tf_op jit(solution)/shard_map/ppermute | solution.py:30
  236.0 10.4 %collective-permute-done.44 = bf16[128,1024]{1,0:T(8,128)(2,1)S(1)} collective-permute-done((bf16[128,1024]{1,0:T(8,128)(2,1)S(1)}, bf16[128,1024]{1,0:T(8,128)(2,1)S(1)}, u32[]{:S(2)}, u32[]{:S(2)}) %collective-permute-start.44) | collective-permute-done | bytes 262176 | tf_op jit(solution)/shard_map/ppermute | solution.py:30
  246.6 8.4 %collective-permute-done.50 = bf16[128,1024]{1,0:T(8,128)(2,1)S(1)} collective-permute-done((bf16[128,1024]{1,0:T(8,128)(2,1)S(1)}, bf16[128,1024]{1,0:T(8,128)(2,1)S(1)}, u32[]{:S(2)}, u32[]{:S(2)}) %collective-permute-start.50) | collective-permute-done | bytes 262176 | tf_op jit(solution)/shard_map/ppermute | solution.py:30
  254.9 4.7 %collective-permute-done.43 = bf16[128,1024]{1,0:T(8,128)(2,1)S(1)} collective-permute-done((bf16[128,1024]{1,0:T(8,128)(2,1)S(1)}, bf16[128,1024]{1,0:T(8,128)(2,1)S(1)}, u32[]{:S(2)}, u32[]{:S(2)}) %collective-permute-start.43) | collective-permute-done | bytes 262176 | tf_op jit(solution)/shard_map/ppermute | solution.py:30
  259.6 5.6 %collective-permute-done.45 = bf16[128,1024]{1,0:T(8,128)(2,1)S(1)} collective-permute-done((bf16[128,1024]{1,0:T(8,128)(2,1)S(1)}, bf16[128,1024]{1,0:T(8,128)(2,1)S(1)}, u32[]{:S(2)}, u32[]{:S(2)}) %collective-permute-start.45) | collective-permute-done | bytes 262176 | tf_op jit(solution)/shard_map/ppermute | solution.py:30
  (178 shorter events, 31.7 us)
Async XLA Ops:
  0.0 12.9 %copy-start.26 = (bf16[1024,128]{1,0:T(8,128)(2,1)S(1)}, bf16[1024,128]{1,0:T(8,128)(2,1)}, u32[]{:S(2)}) copy-start(bf16[1024,128]{1,0:T(8,128)(2,1)} %param.15) | copy-start | bytes 786436
  1.6 19.3 %collective-permute-start.7 = (bf16[128,512]{1,0:T(8,128)(2,1)}, bf16[128,512]{1,0:T(8,128)(2,1)S(1)}, u32[]{:S(2)}, u32[]{:S(2)}) collective-permute-start(bf16[128,512]{1,0:T(8,128)(2,1)} %constant_dynamic-slice_fusion), channel_id=1, source_target_pairs={{0,4},{1,5},{2,6},{3,7},{4,0},{5,1},{6,2},{7,3},{8,12},{9,13},{10,... | collective-permute-start | bytes 393224 | tf_op jit(solution)/shard_map/ppermute | solution.py:30
  5.7 15.8 %collective-permute-start.6 = (bf16[128,512]{1,0:T(8,128)(2,1)}, bf16[128,512]{1,0:T(8,128)(2,1)}, u32[]{:S(2)}, u32[]{:S(2)}) collective-permute-start(bf16[128,512]{1,0:T(8,128)(2,1)} %constant_dynamic-slice_fusion), channel_id=1, source_target_pairs={{0,2},{1,3},{2,0},{3,1},{4,6},{5,7},{6,4},{7,5},{8,10},{9,11},{10,... | collective-permute-start | bytes 393224 | tf_op jit(solution)/shard_map/ppermute | solution.py:30
  8.8 5.0 %collective-permute-start = (bf16[128,128]{0,1:T(8,128)(2,1)S(1)}, bf16[128,128]{0,1:T(8,128)(2,1)S(1)}, u32[]{:S(2)}, u32[]{:S(2)}) collective-permute-start(bf16[128,128]{0,1:T(8,128)(2,1)S(1)} %pad_maximum_fusion.2), channel_id=1, source_target_pairs={{0,8},{8,16},{16,24},{1,9},{9,17},{17,25},{2,10},{10,18},{18,26},{... | collective-permute-start | bytes 98312 | tf_op jit(solution)/shard_map/ppermute | solution.py:23
  16.8 32.7 %copy-start = (bf16[1,768,2048]{2,1,0:T(8,128)(2,1)S(1)}, bf16[1,768,2048]{2,1,0:T(8,128)(2,1)}, u32[]{:S(2)}) copy-start(bf16[1,768,2048]{2,1,0:T(8,128)(2,1)} %param.24) | copy-start | bytes 9437188
  16.8 35.0 %copy-start.25 = (f32[2048]{0:T(1024)S(1)}, f32[2048]{0:T(1024)}, u32[]{:S(2)}) copy-start(f32[2048]{0:T(1024)} %param.21) | copy-start | bytes 24580
  19.6 12.5 %copy-start.3 = (bf16[128,2048]{1,0:T(8,128)(2,1)S(1)}, bf16[128,2048]{1,0:T(8,128)(2,1)}, u32[]{:S(2)}) copy-start(bf16[128,2048]{1,0:T(8,128)(2,1)} %refs_4_.1) | copy-start | bytes 1572868
  19.6 32.2 %copy-start.4 = (bf16[128,2048]{1,0:T(8,128)(2,1)S(1)}, bf16[128,2048]{1,0:T(8,128)(2,1)}, u32[]{:S(2)}) copy-start(bf16[128,2048]{1,0:T(8,128)(2,1)} %refs_14_.1) | copy-start | bytes 1572868
  20.8 10.8 %collective-permute-start.1 = (bf16[512,128]{1,0:T(8,128)(2,1)S(1)}, bf16[512,128]{1,0:T(8,128)(2,1)S(1)}, u32[]{:S(2)}, u32[]{:S(2)}) collective-permute-start(bf16[512,128]{1,0:T(8,128)(2,1)S(1)} %bitcast.106), channel_id=1, source_target_pairs={{0,1},{1,0},{2,3},{3,2},{4,5},{5,4},{6,7},{7,6},{8,9},{9,8},{10,11... | collective-permute-start | bytes 393224 | tf_op jit(solution)/shard_map/ppermute | solution.py:30
  20.9 5.9 %collective-permute-start.8 = (bf16[128,512]{1,0:T(8,128)(2,1)S(1)}, bf16[128,512]{1,0:T(8,128)(2,1)S(1)}, u32[]{:S(2)}, u32[]{:S(2)}) collective-permute-start(bf16[128,512]{1,0:T(8,128)(2,1)S(1)} %collective-permute-done.7), channel_id=1, source_target_pairs={{0,2},{1,3},{2,0},{3,1},{4,6},{5,7},{6,4},{7,5},{8,10},{9,11},{10,... | collective-permute-start | bytes 393224 | tf_op jit(solution)/shard_map/ppermute | solution.py:30
  26.8 21.6 %collective-permute-start.10 = (bf16[384,512]{1,0:T(8,128)(2,1)S(1)}, bf16[384,512]{1,0:T(8,128)(2,1)S(1)}, u32[]{:S(2)}, u32[]{:S(2)}) collective-permute-start(bf16[384,512]{1,0:T(8,128)(2,1)S(1)} %constant_dynamic-update-slice_fusion.refs_6_), channel_id=1, source_target_pairs={{0,8},{8,0},{16,24},{24,16},{1,9},{9,1},{17,25},{25,17},{2,10},{10... | collective-permute-start | bytes 1179656 | tf_op jit(solution)/shard_map/ppermute | solution.py:30
  29.2 19.8 %collective-permute-start.12 = (bf16[384,512]{1,0:T(8,128)(2,1)S(1)}, bf16[384,512]{1,0:T(8,128)(2,1)S(1)}, u32[]{:S(2)}, u32[]{:S(2)}) collective-permute-start(bf16[384,512]{1,0:T(8,128)(2,1)S(1)} %constant_dynamic-update-slice_fusion.refs_6_), channel_id=1, source_target_pairs={{0,16},{8,24},{16,0},{24,8},{1,17},{9,25},{17,1},{25,9},{2,18},{10... | collective-permute-start | bytes 1179656 | tf_op jit(solution)/shard_map/ppermute | solution.py:30
  30.7 18.3 %collective-permute-start.14 = (bf16[384,512]{1,0:T(8,128)(2,1)S(1)}, bf16[384,512]{1,0:T(8,128)(2,1)S(1)}, u32[]{:S(2)}, u32[]{:S(2)}) collective-permute-start(bf16[384,512]{1,0:T(8,128)(2,1)S(1)} %constant_dynamic-update-slice_fusion.refs_6_), channel_id=1, source_target_pairs={{0,24},{8,16},{16,8},{24,0},{1,25},{9,17},{17,9},{25,1},{2,26},{10... | collective-permute-start | bytes 1179656 | tf_op jit(solution)/shard_map/ppermute | solution.py:30
  31.6 4.3 %collective-permute-start.2 = (bf16[128,256]{1,0:T(8,128)(2,1)S(1)}, bf16[128,256]{1,0:T(8,128)(2,1)S(1)}, u32[]{:S(2)}, u32[]{:S(2)}) collective-permute-start(bf16[128,256]{1,0:T(8,128)(2,1)S(1)} %get-tuple-element.91), channel_id=1, source_target_pairs={{0,2},{1,3},{2,0},{3,1},{4,6},{5,7},{6,4},{7,5},{8,10},{9,11},{10,... | collective-permute-start | bytes 196616 | tf_op jit(solution)/shard_map/ppermute | solution.py:30
  32.1 17.3 %collective-permute-start.5 = (bf16[128,2048]{1,0:T(8,128)(2,1)S(1)}, bf16[128,2048]{1,0:T(8,128)(2,1)S(1)}, u32[]{:S(2)}, u32[]{:S(2)}) collective-permute-start(bf16[128,2048]{1,0:T(8,128)(2,1)S(1)} %copy-done.3), channel_id=1, source_target_pairs={{0,1},{1,0},{2,3},{3,2},{4,5},{5,4},{6,7},{7,6},{8,9},{9,8},{10,11... | collective-permute-start | bytes 1572872 | tf_op jit(solution)/shard_map/ppermute | solution.py:30
  36.0 6.4 %collective-permute-start.3 = (bf16[128,256]{1,0:T(8,128)(2,1)S(1)}, bf16[128,256]{1,0:T(8,128)(2,1)S(1)}, u32[]{:S(2)}, u32[]{:S(2)}) collective-permute-start(bf16[128,256]{1,0:T(8,128)(2,1)S(1)} %get-tuple-element.92), channel_id=1, source_target_pairs={{0,4},{1,5},{2,6},{3,7},{4,0},{5,1},{6,2},{7,3},{8,12},{9,13},{10,... | collective-permute-start | bytes 196616 | tf_op jit(solution)/shard_map/ppermute | solution.py:30
  42.4 6.1 %collective-permute-start.4 = (bf16[128,256]{1,0:T(8,128)(2,1)S(1)}, bf16[128,256]{1,0:T(8,128)(2,1)S(1)}, u32[]{:S(2)}, u32[]{:S(2)}) collective-permute-start(bf16[128,256]{1,0:T(8,128)(2,1)S(1)} %get-tuple-element.89), channel_id=1, source_target_pairs={{0,6},{1,7},{2,4},{3,5},{4,2},{5,3},{6,0},{7,1},{8,14},{9,15},{10,... | collective-permute-start | bytes 196616 | tf_op jit(solution)/shard_map/ppermute | solution.py:30
  48.5 1.7 collective-permute-start.9
  48.5 2.3 collective-permute-start.11
  49.0 2.3 collective-permute-start.13
  49.0 2.8 %collective-permute-start.15 = (bf16[384,512]{1,0:T(8,128)(2,1)S(1)}, bf16[384,512]{1,0:T(8,128)(2,1)S(1)}, u32[]{:S(2)}, u32[]{:S(2)}) collective-permute-start(bf16[384,512]{1,0:T(8,128)(2,1)S(1)} %collective-permute-done.14.refs_12_), channel_id=1, source_target_pairs={{0,1},{1,0},{2,3},{3,2},{4,5},{5,4},{6,7},{7,6},{8,9},{9,8},{10,11... | collective-permute-start | bytes 1179656 | tf_op jit(solution)/shard_map/ppermute | solution.py:30
  49.5 103.4 %collective-permute-start.30 = (bf16[768,2048]{1,0:T(8,128)(2,1)S(1)}, bf16[768,2048]{1,0:T(8,128)(2,1)}, u32[]{:S(2)}, u32[]{:S(2)}) collective-permute-start(bf16[768,2048]{1,0:T(8,128)(2,1)S(1)} %bitcast.80), channel_id=1, source_target_pairs={{0,1},{1,0},{2,3},{3,2},{4,5},{5,4},{6,7},{7,6},{8,9},{9,8},{10,11... | collective-permute-start | bytes 9437192 | tf_op jit(solution)/shard_map/ppermute | solution.py:30
  50.2 103.5 %collective-permute-start.31 = (bf16[768,2048]{1,0:T(8,128)(2,1)}, bf16[768,2048]{1,0:T(8,128)(2,1)}, u32[]{:S(2)}, u32[]{:S(2)}) collective-permute-start(bf16[768,2048]{1,0:T(8,128)(2,1)} %bitcast.85), channel_id=1, source_target_pairs={{0,1},{1,0},{2,3},{3,2},{4,5},{5,4},{6,7},{7,6},{8,9},{9,8},{10,11... | collective-permute-start | bytes 9437192 | tf_op jit(solution)/shard_map/ppermute | solution.py:30
  51.9 33.8 %copy-start.28 = (s32[1024,4]{0,1:T(4,128)S(1)}, s32[1024,4]{0,1:T(4,128)}, u32[]{:S(2)}) copy-start(s32[1024,4]{0,1:T(4,128)} %param.22) | copy-start | bytes 49156
  51.9 41.8 %copy-start.29 = (f32[1024,4]{0,1:T(4,128)S(1)}, f32[1024,4]{0,1:T(4,128)}, u32[]{:S(2)}) copy-start(f32[1024,4]{0,1:T(4,128)} %param.23) | copy-start | bytes 49156
  54.0 13.4 %collective-permute-start.24 = (bf16[128,1024]{1,0:T(8,128)(2,1)S(1)}, bf16[128,1024]{1,0:T(8,128)(2,1)}, u32[]{:S(2)}, u32[]{:S(2)}) collective-permute-start(bf16[128,1024]{1,0:T(8,128)(2,1)S(1)} %get-tuple-element.42.refs_1_), channel_id=1, source_target_pairs={{0,4},{1,5},{2,6},{3,7},{4,0},{5,1},{6,2},{7,3},{8,12},{9,13},{10,... | collective-permute-start | bytes 786440 | tf_op jit(solution)/shard_map/ppermute | solution.py:30
  54.0 14.1 %collective-permute-start.23 = (bf16[128,1024]{1,0:T(8,128)(2,1)S(1)}, bf16[128,1024]{1,0:T(8,128)(2,1)S(1)}, u32[]{:S(2)}, u32[]{:S(2)}) collective-permute-start(bf16[128,1024]{1,0:T(8,128)(2,1)S(1)} %get-tuple-element.42.refs_1_), channel_id=1, source_target_pairs={{0,2},{1,3},{2,0},{3,1},{4,6},{5,7},{6,4},{7,5},{8,10},{9,11},{10,... | collective-permute-start | bytes 786440 | tf_op jit(solution)/shard_map/ppermute | solution.py:30
  54.5 100.5 %collective-permute-start.32 = (bf16[768,2048]{1,0:T(8,128)(2,1)}, bf16[768,2048]{1,0:T(8,128)(2,1)}, u32[]{:S(2)}, u32[]{:S(2)}) collective-permute-start(bf16[768,2048]{1,0:T(8,128)(2,1)} %bitcast.41.refs_4_), channel_id=1, source_target_pairs={{0,1},{1,0},{2,3},{3,2},{4,5},{5,4},{6,7},{7,6},{8,9},{9,8},{10,11... | collective-permute-start | bytes 9437192 | tf_op jit(solution)/shard_map/ppermute | solution.py:30
  67.3 1.5 collective-permute-start.26
  68.1 14.5 %collective-permute-start.17 = (bf16[128,1024]{1,0:T(8,128)(2,1)S(1)}, bf16[128,1024]{1,0:T(8,128)(2,1)}, u32[]{:S(2)}, u32[]{:S(2)}) collective-permute-start(bf16[128,1024]{1,0:T(8,128)(2,1)S(1)} %get-tuple-element.40.refs_1_), channel_id=1, source_target_pairs={{0,4},{1,5},{2,6},{3,7},{4,0},{5,1},{6,2},{7,3},{8,12},{9,13},{10,... | collective-permute-start | bytes 786440 | tf_op jit(solution)/shard_map/ppermute | solution.py:30
  69.6 13.9 %collective-permute-start.16 = (bf16[128,1024]{1,0:T(8,128)(2,1)S(1)}, bf16[128,1024]{1,0:T(8,128)(2,1)S(1)}, u32[]{:S(2)}, u32[]{:S(2)}) collective-permute-start(bf16[128,1024]{1,0:T(8,128)(2,1)S(1)} %get-tuple-element.40.refs_1_), channel_id=1, source_target_pairs={{0,2},{1,3},{2,0},{3,1},{4,6},{5,7},{6,4},{7,5},{8,10},{9,11},{10,... | collective-permute-start | bytes 786440 | tf_op jit(solution)/shard_map/ppermute | solution.py:30
  82.5 1.5 collective-permute-start.19
  83.5 7.9 %collective-permute-start.25 = (bf16[128,1024]{1,0:T(8,128)(2,1)}, bf16[128,1024]{1,0:T(8,128)(2,1)S(1)}, u32[]{:S(2)}, u32[]{:S(2)}) collective-permute-start(bf16[128,1024]{1,0:T(8,128)(2,1)} %collective-permute-done.24.refs_3_), channel_id=1, source_target_pairs={{0,2},{1,3},{2,0},{3,1},{4,6},{5,7},{6,4},{7,5},{8,10},{9,11},{10,... | collective-permute-start | bytes 786440 | tf_op jit(solution)/shard_map/ppermute | solution.py:30
  85.0 6.5 %collective-permute-start.27 = (bf16[128,1024]{1,0:T(8,128)(2,1)S(1)}, bf16[128,1024]{1,0:T(8,128)(2,1)S(1)}, u32[]{:S(2)}, u32[]{:S(2)}) collective-permute-start(bf16[128,1024]{1,0:T(8,128)(2,1)S(1)} %collective-permute-done.23.refs_2_), channel_id=1, source_target_pairs={{0,1},{1,0},{2,3},{3,2},{4,5},{5,4},{6,7},{7,6},{8,9},{9,8},{10,11... | collective-permute-start | bytes 786440 | tf_op jit(solution)/shard_map/ppermute | solution.py:30
  91.5 5.3 %collective-permute-start.28 = (bf16[128,1024]{1,0:T(8,128)(2,1)}, bf16[128,1024]{1,0:T(8,128)(2,1)}, u32[]{:S(2)}, u32[]{:S(2)}) collective-permute-start(bf16[128,1024]{1,0:T(8,128)(2,1)} %collective-permute-done.24.refs_3_), channel_id=1, source_target_pairs={{0,1},{1,0},{2,3},{3,2},{4,5},{5,4},{6,7},{7,6},{8,9},{9,8},{10,11... | collective-permute-start | bytes 786440 | tf_op jit(solution)/shard_map/ppermute | solution.py:30
  92.9 8.3 %collective-permute-start.18 = (bf16[128,1024]{1,0:T(8,128)(2,1)}, bf16[128,1024]{1,0:T(8,128)(2,1)}, u32[]{:S(2)}, u32[]{:S(2)}) collective-permute-start(bf16[128,1024]{1,0:T(8,128)(2,1)} %collective-permute-done.17.refs_3_), channel_id=1, source_target_pairs={{0,2},{1,3},{2,0},{3,1},{4,6},{5,7},{6,4},{7,5},{8,10},{9,11},{10,... | collective-permute-start | bytes 786440 | tf_op jit(solution)/shard_map/ppermute | solution.py:30
  96.8 5.6 %collective-permute-start.20 = (bf16[128,1024]{1,0:T(8,128)(2,1)}, bf16[128,1024]{1,0:T(8,128)(2,1)S(1)}, u32[]{:S(2)}, u32[]{:S(2)}) collective-permute-start(bf16[128,1024]{1,0:T(8,128)(2,1)} %copy-done.9), channel_id=1, source_target_pairs={{0,1},{1,0},{2,3},{3,2},{4,5},{5,4},{6,7},{7,6},{8,9},{9,8},{10,11... | collective-permute-start | bytes 786440 | tf_op jit(solution)/shard_map/ppermute | solution.py:30
  101.2 2.3 collective-permute-start.29
  103.1 20.7 %collective-permute-start.21 = (bf16[128,1024]{1,0:T(8,128)(2,1)}, bf16[128,1024]{1,0:T(8,128)(2,1)}, u32[]{:S(2)}, u32[]{:S(2)}) collective-permute-start(bf16[128,1024]{1,0:T(8,128)(2,1)} %collective-permute-done.17.refs_3_), channel_id=1, source_target_pairs={{0,1},{1,0},{2,3},{3,2},{4,5},{5,4},{6,7},{7,6},{8,9},{9,8},{10,11... | collective-permute-start | bytes 786440 | tf_op jit(solution)/shard_map/ppermute | solution.py:30
  104.3 21.7 %collective-permute-start.22 = (bf16[128,1024]{1,0:T(8,128)(2,1)}, bf16[128,1024]{1,0:T(8,128)(2,1)}, u32[]{:S(2)}, u32[]{:S(2)}) collective-permute-start(bf16[128,1024]{1,0:T(8,128)(2,1)} %collective-permute-done.18.refs_4_), channel_id=1, source_target_pairs={{0,1},{1,0},{2,3},{3,2},{4,5},{5,4},{6,7},{7,6},{8,9},{9,8},{10,11... | collective-permute-start | bytes 786440 | tf_op jit(solution)/shard_map/ppermute | solution.py:30
  118.8 7.2 %copy-start.22 = (bf16[128,1024]{1,0:T(8,128)(2,1)S(1)}, bf16[128,1024]{1,0:T(8,128)(2,1)}, u32[]{:S(2)}) copy-start(bf16[128,1024]{1,0:T(8,128)(2,1)} %copy-done.21) | copy-start | bytes 786436
  123.8 15.8 %collective-permute-start.40 = (bf16[256,1024]{1,0:T(8,128)(2,1)S(1)}, bf16[256,1024]{1,0:T(8,128)(2,1)S(1)}, u32[]{:S(2)}, u32[]{:S(2)}) collective-permute-start(bf16[256,1024]{1,0:T(8,128)(2,1)S(1)} %get-tuple-element.52), channel_id=1, source_target_pairs={{0,24},{1,25},{2,26},{3,27},{4,28},{5,29},{6,30},{7,31},{8,16},{9,... | collective-permute-start | bytes 1572872 | tf_op jit(solution)/shard_map/ppermute | solution.py:424
  126.0 26.8 %copy-start.27 = (bf16[64,2048]{1,0:T(8,128)(2,1)S(1)}, bf16[64,2048]{1,0:T(8,128)(2,1)}, u32[]{:S(2)}) copy-start(bf16[64,2048]{1,0:T(8,128)(2,1)} %param.29) | copy-start | bytes 786436
  126.1 29.0 %copy-start.1 = (bf16[1,768,2048]{2,1,0:T(8,128)(2,1)S(1)}, bf16[1,768,2048]{2,1,0:T(8,128)(2,1)}, u32[]{:S(2)}) copy-start(bf16[1,768,2048]{2,1,0:T(8,128)(2,1)} %param.25) | copy-start | bytes 9437188
  131.3 19.6 %collective-permute-start.39 = (bf16[256,1024]{1,0:T(8,128)(2,1)S(1)}, bf16[256,1024]{1,0:T(8,128)(2,1)S(1)}, u32[]{:S(2)}, u32[]{:S(2)}) collective-permute-start(bf16[256,1024]{1,0:T(8,128)(2,1)S(1)} %get-tuple-element.51), channel_id=1, source_target_pairs={{0,24},{1,25},{2,26},{3,27},{4,28},{5,29},{6,30},{7,31},{8,16},{9,... | collective-permute-start | bytes 1572872 | tf_op jit(solution)/shard_map/ppermute | solution.py:424
  139.6 23.3 %collective-permute-start.37 = (bf16[256,1024]{1,0:T(8,128)(2,1)S(1)}, bf16[256,1024]{1,0:T(8,128)(2,1)S(1)}, u32[]{:S(2)}, u32[]{:S(2)}) collective-permute-start(bf16[256,1024]{1,0:T(8,128)(2,1)S(1)} %get-tuple-element.49), channel_id=1, source_target_pairs={{0,16},{1,9},{2,18},{3,11},{4,20},{5,13},{6,22},{7,15},{8,24},{9,1... | collective-permute-start | bytes 1572872 | tf_op jit(solution)/shard_map/ppermute | solution.py:424
  150.8 21.1 %collective-permute-start.36 = (bf16[256,1024]{1,0:T(8,128)(2,1)S(1)}, bf16[256,1024]{1,0:T(8,128)(2,1)S(1)}, u32[]{:S(2)}, u32[]{:S(2)}) collective-permute-start(bf16[256,1024]{1,0:T(8,128)(2,1)S(1)} %get-tuple-element.48), channel_id=1, source_target_pairs={{0,16},{1,9},{2,18},{3,11},{4,20},{5,13},{6,22},{7,15},{8,24},{9,1... | collective-permute-start | bytes 1572872 | tf_op jit(solution)/shard_map/ppermute | solution.py:424
  152.9 29.4 %collective-permute-start.34 = (bf16[256,1024]{1,0:T(8,128)(2,1)S(1)}, bf16[256,1024]{1,0:T(8,128)(2,1)S(1)}, u32[]{:S(2)}, u32[]{:S(2)}) collective-permute-start(bf16[256,1024]{1,0:T(8,128)(2,1)S(1)} %get-tuple-element.46), channel_id=1, source_target_pairs={{0,8},{1,17},{2,10},{3,19},{4,12},{5,21},{6,14},{7,23},{8,0},{9,25... | collective-permute-start | bytes 1572872 | tf_op jit(solution)/shard_map/ppermute | solution.py:424
  153.7 28.7 %collective-permute-start.33 = (bf16[256,1024]{1,0:T(8,128)(2,1)S(1)}, bf16[256,1024]{1,0:T(8,128)(2,1)S(1)}, u32[]{:S(2)}, u32[]{:S(2)}) collective-permute-start(bf16[256,1024]{1,0:T(8,128)(2,1)S(1)} %get-tuple-element.45), channel_id=1, source_target_pairs={{0,8},{1,17},{2,10},{3,19},{4,12},{5,21},{6,14},{7,23},{8,0},{9,25... | collective-permute-start | bytes 1572872 | tf_op jit(solution)/shard_map/ppermute | solution.py:424
  162.3 31.1 %collective-permute-start.48 = (bf16[256,1024]{1,0:T(8,128)(2,1)S(1)}, bf16[256,1024]{1,0:T(8,128)(2,1)S(1)}, u32[]{:S(2)}, u32[]{:S(2)}) collective-permute-start(bf16[256,1024]{1,0:T(8,128)(2,1)S(1)} %get-tuple-element.66), channel_id=1, source_target_pairs={{0,24},{1,25},{2,26},{3,27},{4,28},{5,29},{6,30},{7,31},{8,16},{9,... | collective-permute-start | bytes 1572872 | tf_op jit(solution)/shard_map/ppermute | solution.py:424
  179.4 22.0 %collective-permute-start.47 = (bf16[256,1024]{1,0:T(8,128)(2,1)S(1)}, bf16[256,1024]{1,0:T(8,128)(2,1)S(1)}, u32[]{:S(2)}, u32[]{:S(2)}) collective-permute-start(bf16[256,1024]{1,0:T(8,128)(2,1)S(1)} %get-tuple-element.65), channel_id=1, source_target_pairs={{0,16},{1,9},{2,18},{3,11},{4,20},{5,13},{6,22},{7,15},{8,24},{9,1... | collective-permute-start | bytes 1572872 | tf_op jit(solution)/shard_map/ppermute | solution.py:424
  189.7 14.9 %collective-permute-start.46 = (bf16[256,1024]{1,0:T(8,128)(2,1)S(1)}, bf16[256,1024]{1,0:T(8,128)(2,1)S(1)}, u32[]{:S(2)}, u32[]{:S(2)}) collective-permute-start(bf16[256,1024]{1,0:T(8,128)(2,1)S(1)} %get-tuple-element.64), channel_id=1, source_target_pairs={{0,8},{1,17},{2,10},{3,19},{4,12},{5,21},{6,14},{7,23},{8,0},{9,25... | collective-permute-start | bytes 1572872 | tf_op jit(solution)/shard_map/ppermute | solution.py:424
  189.9 23.7 %collective-permute-start.41 = (bf16[256,1024]{1,0:T(8,128)(2,1)S(1)}, bf16[256,1024]{1,0:T(8,128)(2,1)S(1)}, u32[]{:S(2)}, u32[]{:S(2)}) collective-permute-start(bf16[256,1024]{1,0:T(8,128)(2,1)S(1)} %get-tuple-element.53), channel_id=1, source_target_pairs={{0,24},{1,25},{2,26},{3,27},{4,28},{5,29},{6,30},{7,31},{8,16},{9,... | collective-permute-start | bytes 1572872 | tf_op jit(solution)/shard_map/ppermute | solution.py:424
  191.5 26.8 %collective-permute-start.38 = (bf16[256,1024]{1,0:T(8,128)(2,1)S(1)}, bf16[256,1024]{1,0:T(8,128)(2,1)S(1)}, u32[]{:S(2)}, u32[]{:S(2)}) collective-permute-start(bf16[256,1024]{1,0:T(8,128)(2,1)S(1)} %get-tuple-element.50), channel_id=1, source_target_pairs={{0,16},{1,9},{2,18},{3,11},{4,20},{5,13},{6,22},{7,15},{8,24},{9,1... | collective-permute-start | bytes 1572872 | tf_op jit(solution)/shard_map/ppermute | solution.py:424
  193.4 25.0 %collective-permute-start.35 = (bf16[256,1024]{1,0:T(8,128)(2,1)S(1)}, bf16[256,1024]{1,0:T(8,128)(2,1)S(1)}, u32[]{:S(2)}, u32[]{:S(2)}) collective-permute-start(bf16[256,1024]{1,0:T(8,128)(2,1)S(1)} %get-tuple-element.47), channel_id=1, source_target_pairs={{0,8},{1,17},{2,10},{3,19},{4,12},{5,21},{6,14},{7,23},{8,0},{9,25... | collective-permute-start | bytes 1572872 | tf_op jit(solution)/shard_map/ppermute | solution.py:424
  206.3 19.5 %collective-permute-start.49 = (bf16[512,1024]{1,0:T(8,128)(2,1)S(1)}, bf16[512,1024]{1,0:T(8,128)(2,1)S(1)}, u32[]{:S(2)}, u32[]{:S(2)}) collective-permute-start(bf16[512,1024]{1,0:T(8,128)(2,1)S(1)} %combine.7), channel_id=1, source_target_pairs={{0,1},{1,0},{2,3},{3,2},{4,5},{5,4},{6,7},{7,6},{8,9},{9,8},{10,11... | collective-permute-start | bytes 3145736 | tf_op jit(solution)/shard_map/ppermute | solution.py:30
  220.3 6.0 %collective-permute-start.42 = (bf16[512,1024]{1,0:T(8,128)(2,1)S(1)}, bf16[512,1024]{1,0:T(8,128)(2,1)S(1)}, u32[]{:S(2)}, u32[]{:S(2)}) collective-permute-start(bf16[512,1024]{1,0:T(8,128)(2,1)S(1)} %combine.5), channel_id=1, source_target_pairs={{0,1},{1,0},{2,3},{3,2},{4,5},{5,4},{6,7},{7,6},{8,9},{9,8},{10,11... | collective-permute-start | bytes 3145736 | tf_op jit(solution)/shard_map/ppermute | solution.py:30
  225.9 9.2 %collective-permute-start.51 = (bf16[128,1024]{1,0:T(8,128)(2,1)S(1)}, bf16[128,1024]{1,0:T(8,128)(2,1)S(1)}, u32[]{:S(2)}, u32[]{:S(2)}) collective-permute-start(bf16[128,1024]{1,0:T(8,128)(2,1)S(1)} %get-tuple-element.80), channel_id=1, source_target_pairs={{0,2},{1,3},{2,0},{3,1},{4,6},{5,7},{6,4},{7,5},{8,10},{9,11},{10,... | collective-permute-start | bytes 786440 | tf_op jit(solution)/shard_map/ppermute | solution.py:30
  226.3 38.9 %copy-start.6 = (bf16[128,2048]{1,0:T(8,128)(2,1)S(1)}, bf16[128,2048]{1,0:T(8,128)(2,1)}, u32[]{:S(2)}) copy-start(bf16[128,2048]{1,0:T(8,128)(2,1)} %copy-done.5) | copy-start | bytes 1572868
  226.4 20.0 %collective-permute-start.44 = (bf16[128,1024]{1,0:T(8,128)(2,1)S(1)}, bf16[128,1024]{1,0:T(8,128)(2,1)S(1)}, u32[]{:S(2)}, u32[]{:S(2)}) collective-permute-start(bf16[128,1024]{1,0:T(8,128)(2,1)S(1)} %get-tuple-element.78), channel_id=1, source_target_pairs={{0,2},{1,3},{2,0},{3,1},{4,6},{5,7},{6,4},{7,5},{8,10},{9,11},{10,... | collective-permute-start | bytes 786440 | tf_op jit(solution)/shard_map/ppermute | solution.py:30
  228.2 26.7 %collective-permute-start.50 = (bf16[128,1024]{1,0:T(8,128)(2,1)S(1)}, bf16[128,1024]{1,0:T(8,128)(2,1)S(1)}, u32[]{:S(2)}, u32[]{:S(2)}) collective-permute-start(bf16[128,1024]{1,0:T(8,128)(2,1)S(1)} %get-tuple-element.79), channel_id=1, source_target_pairs={{0,2},{1,3},{2,0},{3,1},{4,6},{5,7},{6,4},{7,5},{8,10},{9,11},{10,... | collective-permute-start | bytes 786440 | tf_op jit(solution)/shard_map/ppermute | solution.py:30
  228.5 31.1 %collective-permute-start.43 = (bf16[128,1024]{1,0:T(8,128)(2,1)S(1)}, bf16[128,1024]{1,0:T(8,128)(2,1)S(1)}, u32[]{:S(2)}, u32[]{:S(2)}) collective-permute-start(bf16[128,1024]{1,0:T(8,128)(2,1)S(1)} %get-tuple-element.77), channel_id=1, source_target_pairs={{0,2},{1,3},{2,0},{3,1},{4,6},{5,7},{6,4},{7,5},{8,10},{9,11},{10,... | collective-permute-start | bytes 786440 | tf_op jit(solution)/shard_map/ppermute | solution.py:30
  235.3 24.4 %collective-permute-start.52 = (bf16[128,1024]{1,0:T(8,128)(2,1)S(1)}, bf16[128,1024]{1,0:T(8,128)(2,1)S(1)}, u32[]{:S(2)}, u32[]{:S(2)}) collective-permute-start(bf16[128,1024]{1,0:T(8,128)(2,1)S(1)} %add_convert_fusion.1), channel_id=1, source_target_pairs={{0,4},{1,5},{2,6},{3,7},{4,0},{5,1},{6,2},{7,3},{8,12},{9,13},{10,... | collective-permute-start | bytes 786440 | tf_op jit(solution)/shard_map/ppermute | solution.py:30
  246.5 18.7 %collective-permute-start.45 = (bf16[128,1024]{1,0:T(8,128)(2,1)S(1)}, bf16[128,1024]{1,0:T(8,128)(2,1)S(1)}, u32[]{:S(2)}, u32[]{:S(2)}) collective-permute-start(bf16[128,1024]{1,0:T(8,128)(2,1)S(1)} %add_convert_fusion.5), channel_id=1, source_target_pairs={{0,4},{1,5},{2,6},{3,7},{4,0},{5,1},{6,2},{7,3},{8,12},{9,13},{10,... | collective-permute-start | bytes 786440 | tf_op jit(solution)/shard_map/ppermute | solution.py:30
  (20 other events, 29.9 us)
